TPU v7x, 32 devices: a whole 2x2x4 slice. The times are simulated.
32 devices in a mesh: grp: 2 (over x), sp: 4 (over y, core), tp: 4 (over z).
Axes of the slice: x: 2, y: 2, z: 4, core: 2. Of those that a mesh axis runs over, the one named last changes fastest.
Arguments:
- resid_in: bfloat16 [4096, 2048], P(('grp', 'sp', 'tp')), parts along dimension 0, may hold values from -6 to 6
- pool_input: bfloat16 [4096, 1024], P(('grp', 'sp'), 'tp'), parts along dimension 0, may hold values from -6 to 6
- pool_weight: bfloat16 [4, 256, 256], replicated, may hold values from -0.375 to 0.375
- pool_scale: float32 [1024], replicated, may hold values from 0.2 to 0.8
- out_weight: bfloat16 [1024, 2048], replicated, may hold values from -0.1875 to 0.1875
- mix_gain: float32 [2048], replicated, may hold values from 0.1 to 1.9
- ffn_gain: float32 [2048], replicated, may hold values from 0.1 to 1.9
- w_gate: bfloat16 [32, 2048, 1024], P('sp', None, 'tp'), may hold values from -0.375 to 0.375
- w_up: bfloat16 [32, 2048, 1024], P('sp', None, 'tp'), may hold values from -0.375 to 0.375
- w_down: bfloat16 [32, 1024, 2048], P('sp', 'tp'), may hold values from -0.1875 to 0.1875
- routes: int32 [4096, 2], P(('grp', 'sp', 'tp')), parts along dimension 0, may hold values from 0 to 31, all different within a row; in each aligned block of 128 rows (0 to 127, 128 to 255, ...) at most 9 rows name the same one
- route_weight: float32 [4096, 2], P(('grp', 'sp', 'tp')), parts along dimension 0, may hold values from 0.1 to 1
- post_gain: float32 [2048], replicated, may hold values from 0.1 to 1.9
Outputs:
- layer_out: bfloat16 [4096, 2048], P(('grp', 'sp', 'tp')), parts along dimension 0
There are 2 independent parts, one for each index of `grp`. A program takes and returns all parts, laid end to end along the dimension named above; an argument that names none is the same for every part. Nothing has to cross between parts.
Inputs may be any that keep to these rules, and one draw needn't show every extreme that they name: `routes`: each row names 2 different experts. The rows of one device name any one expert at most 9 times, and in every draw some device's rows name some expert exactly 9 times.
All inputs are finite; a program needn't handle non-finite values.
Results may differ from a plain program's by a relative error of at most 0.011.
Values may be sent and summed in bfloat16 or wider, within the bound.
A program may use at most 128 MiB of HBM per device.

v0:
```python
import functools

import jax
import jax.numpy as jnp
from jax import lax
from jax.experimental import pallas as pl
from jax.experimental.pallas import tpu as pltpu
from jax.sharding import PartitionSpec as P

GROUPS = 4
GROUP_DIM = 256
TOP = 2
CAP = 9


pool_windows = (2, 4, 8, 16)
reach_back = 15
norm_eps = 1e-06
clamp_limit = 7.0
glu_alpha = 1.702


def passed_along(x, axis, by):
    size = lax.axis_size(axis)
    pairs = [(i, i + by) for i in range(size) if 0 <= i + by < size]
    return lax.ppermute(x, axis, pairs)


def rms_scale(values, gain_vec):
    inverse = lax.rsqrt(jnp.mean(values * values, axis=-1, keepdims=True) + norm_eps)
    return values * inverse * gain_vec


def clamped_unit(gate_pre, upward):
    gate_clip = jnp.minimum(gate_pre, clamp_limit)
    linear = jnp.clip(upward, -clamp_limit, clamp_limit)
    return gate_clip * jax.nn.sigmoid(glu_alpha * gate_clip) * (linear + 1.0)


SLOT = 16
Y_FIRST = 16
Z_PART = 64
MESH = pl.DeviceIdType.MESH


def coords():
    return lax.axis_index("grp"), lax.axis_index("sp"), lax.axis_index("tp")


def exchange_kernel(n_tp, pool_ref, out_ref, send, recv, hsend, hrecv, own):
    grp, sp, tp = coords()
    seg_rows = pool_ref.shape[0]
    tok, reach = seg_rows // n_tp, SLOT
    first = tp == 0
    others = [(a, b) for a in range(4) for b in range(n_tp) if (a, b) != (0, 0)]
    barrier = pltpu.get_barrier_semaphore()
    for by in others:
        target = (grp, (sp + by[0]) % 4, (tp + by[1]) % n_tp)
        pl.semaphore_signal(barrier, inc=1, device_id=target, device_id_type=MESH)

    def ends(to, whole, chan):
        if whole:
            at = pl.multiple_of(to * tok - reach, reach)
            return pool_ref.at[pl.ds(at, tok + reach)], out_ref.at[chan]
        return pool_ref.at[pl.ds(0, tok)], out_ref.at[chan, pl.ds(reach, tok)]

    def main(by, whole):
        to = (tp + by) % n_tp
        src, dst = ends(to, whole, tp)
        return pltpu.make_async_remote_copy(
            src_ref=src, dst_ref=dst, send_sem=send.at[by], recv_sem=recv.at[tp],
            device_id=(grp, sp, to), device_id_type=MESH)

    def arrival(by, whole):
        chan = (tp + by) % n_tp
        src, dst = ends(1 if whole else 0, whole, chan)
        return pltpu.make_async_remote_copy(
            src_ref=src, dst_ref=dst, send_sem=send.at[by], recv_sem=recv.at[chan],
            device_id=(grp, sp, chan), device_id_type=MESH)

    def halo(chan):
        return pltpu.make_async_remote_copy(
            src_ref=pool_ref.at[pl.ds(seg_rows - reach, reach)],
            dst_ref=out_ref.at[chan, pl.ds(0, reach)],
            send_sem=hsend.at[0], recv_sem=hrecv.at[chan],
            device_id=(grp, sp + 1, 0), device_id_type=MESH)

    def kept(whole):
        src, dst = ends(tp, whole, tp)
        return pltpu.make_async_copy(src, dst, own.at[0])

    pl.semaphore_wait(barrier, len(others))
    rest = jnp.logical_not(first)
    has_next = sp + 1 < 4
    pl.when(has_next)(lambda: halo(tp).start())
    for by in range(1, n_tp):
        to_first = (tp + by) % n_tp == 0
        pl.when(to_first)(lambda by=by: main(by, False).start())
        pl.when(jnp.logical_not(to_first))(lambda by=by: main(by, True).start())
    pl.when(first)(lambda: kept(False).start())
    pl.when(rest)(lambda: kept(True).start())

    @pl.when(jnp.logical_and(first, sp == 0))
    def _():
        for chan in range(n_tp):
            out_ref[chan, pl.ds(0, reach)] = jnp.zeros((reach, out_ref.shape[2]), out_ref.dtype)

    pl.when(first)(lambda: kept(False).wait())
    pl.when(rest)(lambda: kept(True).wait())
    for by in range(1, n_tp):
        pl.when(first)(lambda by=by: arrival(by, False).wait_recv())
        pl.when(rest)(lambda by=by: arrival(by, True).wait_recv())

    @pl.when(jnp.logical_and(first, sp > 0))
    def _():
        for chan in range(n_tp):
            halo(chan).wait_recv()

    pl.when(has_next)(lambda: halo(tp).wait_send())
    for by in range(1, n_tp):
        to_first = (tp + by) % n_tp == 0
        pl.when(to_first)(lambda by=by: main(by, False).wait_send())
        pl.when(jnp.logical_not(to_first))(lambda by=by: main(by, True).wait_send())


def mixed_tokens(pool_input, pool_weight, pool_scale, n_tp):
    seg_rows, channels = pool_input.shape
    tok = seg_rows // n_tp
    vmem = pl.BlockSpec(memory_space=pltpu.VMEM)
    dma = pltpu.SemaphoreType.DMA
    rows = pl.pallas_call(
        functools.partial(exchange_kernel, n_tp),
        out_shape=jax.ShapeDtypeStruct((n_tp, tok + SLOT, channels), pool_input.dtype),
        in_specs=[vmem],
        out_specs=vmem,
        scratch_shapes=[dma((n_tp,)), dma((n_tp,)), dma((1,)), dma((n_tp,)), dma((1,))],
        compiler_params=pltpu.CompilerParams(collective_id=1, has_side_effects=True),
        name="pool_exchange",
    )(pool_input)
    start = (lax.axis_index("sp") * n_tp + lax.axis_index("tp")) * tok
    count = start + lax.broadcasted_iota(jnp.int32, (tok, 1), 0) + 1
    pooled = []
    for group, window in enumerate(pool_windows):
        held = rows[group].astype(jnp.float32)
        total = held[SLOT:]
        for offset in range(1, window):
            total = total + held[SLOT - offset : SLOT - offset + tok]
        divisor = jnp.minimum(count, window).astype(jnp.float32)
        mixed = (total / divisor - held[SLOT:]).astype(jnp.bfloat16)
        product = jnp.dot(mixed, pool_weight[group], preferred_element_type=jnp.float32)
        scale = pool_scale[group * GROUP_DIM : (group + 1) * GROUP_DIM]
        pooled.append((product * scale).astype(jnp.bfloat16))
    return jnp.concatenate(pooled, axis=1)


def routed_pool(pool_input, pool_weight, pool_scale):
    n_tp = lax.axis_size("tp")
    seg_rows, channels = pool_input.shape
    last_rows = pool_input[seg_rows - reach_back :]
    before = passed_along(last_rows, "sp", 1)
    extended = jnp.concatenate([before, pool_input], axis=0).astype(jnp.float32)
    first_chan = lax.axis_index("tp") * channels
    chan_group = (first_chan + lax.iota(jnp.int32, channels)) // GROUP_DIM
    positions = lax.axis_index("sp") * seg_rows + lax.iota(jnp.int32, seg_rows)
    window = jnp.zeros((channels,), jnp.int32)
    for group_level, win_len in enumerate(pool_windows):
        window = jnp.where(chan_group == group_level, win_len, window)
    running = jnp.zeros((seg_rows, channels), jnp.float32)
    window_sum = running
    for offset in range(pool_windows[-1]):
        running = running + extended[reach_back - offset : reach_back - offset + seg_rows]
        if offset + 1 in pool_windows:
            window_sum = jnp.where(window[None, :] == offset + 1, running, window_sum)
    divisor = jnp.minimum(positions[:, None] + 1, window[None, :]).astype(jnp.float32)
    mixed_rows = (window_sum / divisor - extended[reach_back:]).astype(jnp.bfloat16)
    token_mixed = lax.all_to_all(mixed_rows, "tp", split_axis=0, concat_axis=1, tiled=True)
    tok_rows = token_mixed.shape[0]
    pooled = jnp.einsum(
        "tgc,gcd->tgd",
        token_mixed.reshape(tok_rows, GROUPS, GROUP_DIM),
        pool_weight,
        preferred_element_type=jnp.float32,
    )
    pooled = (
        (pooled * pool_scale.reshape(GROUPS, GROUP_DIM)).astype(jnp.bfloat16).reshape(tok_rows, -1)
    )
    return pooled


def layer_kernel(n_tp, cuts, row_ref, meta_ref, wg_ref, wu_ref, wd_ref, out_ref,
                 every, metas, picks, weights, held, wg, wu, wd,
                 work, from_core, za, zb, ya, yb,
                 send, recv, msend, mrecv, wsem,
                 csend, crecv, asend, arecv, bsend, brecv, ysend, yrecv, own):
    grp, sp, tp = coords()
    yy, core = sp // 2, sp % 2
    yo = 1 - yy
    y_other = yo * 2 + core
    c_other = yy * 2 + (1 - core)
    tok, width = row_ref.shape
    local_experts, buffers = wg_ref.shape[0], wg.shape[0]
    slots = local_experts * SLOT
    chunk = min(1024, width)
    others = [(a, b) for a in range(4) for b in range(n_tp) if (a, b) != (0, 0)]

    def weight_copies(e):
        at = lax.rem(e, buffers)
        return [pltpu.make_async_copy(w.at[e], buf.at[at], wsem.at[i, at])
                for i, (w, buf) in enumerate(((wg_ref, wg), (wu_ref, wu), (wd_ref, wd)))]

    own_copy = pltpu.make_async_copy(row_ref, every.at[sp, tp], own.at[0, 0])
    own_copy.start()
    own_meta = pltpu.make_async_copy(meta_ref, metas.at[sp, tp], own.at[0, 1])
    own_meta.start()
    barrier = pltpu.get_barrier_semaphore()
    for by in others:
        target = (grp, (sp + by[0]) % 4, (tp + by[1]) % n_tp)
        pl.semaphore_signal(barrier, inc=1, device_id=target, device_id_type=MESH)
    pl.semaphore_wait(barrier, len(others))

    def meta_copy(number, by):
        return pltpu.make_async_remote_copy(
            src_ref=meta_ref, dst_ref=metas.at[sp, tp],
            send_sem=msend.at[number], recv_sem=mrecv.at[number],
            device_id=(grp, (sp + by[0]) % 4, (tp + by[1]) % n_tp), device_id_type=MESH)

    own_copy.wait()
    own_meta.wait()

    def copy(s, t, part, way):
        target = [(grp, sp, tp + 1), (grp, sp, tp - 1), (grp, y_other, tp), (grp, c_other, tp)][way]
        first, count = cuts[part]
        piece = every.at[s, t, pl.ds(first, count)]
        return pltpu.make_async_remote_copy(
            src_ref=piece, dst_ref=piece,
            send_sem=send.at[s, t, part, way], recv_sem=recv.at[s, t, part],
            device_id=target, device_id_type=MESH)

    def arrived(s, t, part):
        copy(s, t, part, 3).wait_recv()

    sent = []

    def push(cond, s, t, part, way):
        if way == 0:
            cond = jnp.logical_and(cond, tp + 1 < n_tp)
        if way == 1:
            cond = jnp.logical_and(cond, tp > 0)
        pl.when(cond)(lambda: copy(s, t, part, way).start())
        sent.append((cond, s, t, part, way))

    def source_rows(s, t):
        return pl.ds(pl.multiple_of((s * n_tp + t) * SLOT, SLOT), SLOT)

    def select(s, t):
        slot = lax.broadcasted_iota(jnp.int32, (slots, tok), 0).astype(jnp.float32)
        base = (sp * slots).astype(jnp.float32)
        meta = metas[s, t]
        pick = jnp.zeros((slots, tok), jnp.float32)
        weight = jnp.zeros((slots, tok), jnp.float32)
        for k in range(TOP):
            hit = (meta[k : k + 1] - base) == slot
            pick = pick + jnp.where(hit, 1.0, 0.0)
            weight = weight + jnp.where(hit, meta[TOP + k : TOP + k + 1], 0.0)
        weight = jnp.broadcast_to(jnp.sum(weight, axis=1, keepdims=True), (slots, 128))
        pick = pick.astype(jnp.bfloat16)
        picks[s, t] = pick
        for e in range(local_experts):
            weights[e, source_rows(s, t)] = weight[e * SLOT : (e + 1) * SLOT]

        def body(i, carry):
            at = pl.ds(pl.multiple_of(i * chunk, chunk), chunk)
            got = jnp.dot(pick, every[s, t, :, at], preferred_element_type=jnp.float32)
            got = got.astype(jnp.bfloat16)
            for e in range(local_experts):
                held[e, source_rows(s, t), at] = got[e * SLOT : (e + 1) * SLOT]
            return carry

        lax.fori_loop(0, width // chunk, body, 0)

    yes = tp >= 0
    for number, by in enumerate(others):
        meta_copy(number, by).start()
    push(yes, sp, tp, 0, 2)
    for part in (1, 2):
        push(yes, sp, tp, part, 0)
        push(yes, sp, tp, part, 1)
        push(yes, sp, tp, part, 2)
    push(yes, sp, tp, 0, 0)
    push(yes, sp, tp, 0, 1)
    for part in (0, 1, 2):
        push(yes, sp, tp, part, 3)
    for e in range(min(buffers, local_experts)):
        for c in weight_copies(e):
            c.start()
    arrived(y_other, tp, 0)
    push(yes, y_other, tp, 0, 0)
    push(yes, y_other, tp, 0, 1)
    push(yes, y_other, tp, 0, 3)
    select(sp, tp)
    for number, by in enumerate(others):
        meta_copy(number, by).wait()

    def sides(dist):
        if dist == 0:
            return ((tp, yes),)
        return ((tp - dist, tp >= dist), (tp + dist, tp + dist < n_tp))

    def over_y(dist):
        for t, cond in sides(dist):
            for part in (1, 2):
                pl.when(cond)(functools.partial(arrived, y_other, t, part))
                push(cond, y_other, t, part, 3)
            pl.when(cond)(functools.partial(select, y_other, t))

    def cross(s, t):
        for part in (0, 1, 2):
            arrived(s, t, part)
        select(s, t)

    def over_core(s, dist):
        for t, cond in sides(dist):
            pl.when(cond)(functools.partial(cross, s, t))

    far_core = yo * 2 + (1 - core)
    for dist in range(1, n_tp):
        for s, part in ((sp, 1), (sp, 2), (sp, 0), (y_other, 0)):
            for way, (t, cond) in enumerate(sides(dist)):
                pl.when(cond)(functools.partial(arrived, s, t, part))
                push(cond, s, t, part, way)
                if part:
                    push(cond, s, t, part, 2)
                push(cond, s, t, part, 3)
        for t, cond in sides(dist):
            pl.when(cond)(functools.partial(select, sp, t))
        over_core(c_other, dist - 1)
        over_y(dist - 1)
        if dist > 1:
            over_core(far_core, dist - 2)
    over_core(c_other, n_tp - 1)
    if n_tp > 1:
        over_core(far_core, n_tp - 2)
    over_y(n_tp - 1)
    over_core(far_core, n_tp - 1)
    for cond, s, t, part, way in sent:
        pl.when(cond)(lambda s=s, t=t, part=part, way=way: copy(s, t, part, way).wait_send())

    def expert(e, carry):
        at = lax.rem(e, buffers)
        for c in weight_copies(e):
            c.wait()
        rows = held[e]
        gate_pre = jnp.dot(rows, wg[at], preferred_element_type=jnp.float32)
        upward = jnp.dot(rows, wu[at], preferred_element_type=jnp.float32)
        scale = jnp.concatenate([weights[e]] * (gate_pre.shape[1] // 128), axis=1)
        activated = (clamped_unit(gate_pre, upward) * scale).astype(jnp.bfloat16)

        def down(i, inner):
            cols = pl.ds(pl.multiple_of(i * chunk, chunk), chunk)
            term = jnp.dot(activated, wd[at, :, cols], preferred_element_type=jnp.float32)
            held[e, :, cols] = term.astype(jnp.bfloat16)
            return inner

        lax.fori_loop(0, width // chunk, down, 0)

        @pl.when(e + buffers < local_experts)
        def _():
            for c in weight_copies(e + buffers):
                c.start()

        return carry

    lax.fori_loop(0, local_experts, expert, 0)

    def combined(s, t, at):
        term = held[:, source_rows(s, t), at].reshape(slots, chunk)
        return lax.dot_general(picks[s, t], term, (((0,), (0,)), ((), ())),
                               preferred_element_type=jnp.float32)

    rows_of = [pl.ds(first, count) for first, count in cuts]
    rows_a = rows_of[0]
    ups, downs = (grp, sp, tp + 1), (grp, sp, tp - 1)
    up_ok, down_ok = tp + 1 < n_tp, tp > 0

    def remote(src, dst, s_sem, r_sem, target):
        return pltpu.make_async_remote_copy(
            src_ref=src, dst_ref=dst, send_sem=s_sem, recv_sem=r_sem,
            device_id=target, device_id_type=MESH)

    def core_copy(y, t):
        return remote(every.at[y * 2 + (1 - core), t], from_core.at[y, t],
                      csend.at[y, t], crecv.at[y, t], (grp, c_other, tp))

    def combine_away(y, t):
        s = y * 2 + (1 - core)

        def body(i, carry):
            at = pl.ds(pl.multiple_of(i * chunk, chunk), chunk)
            every[s, t, :, at] = combined(s, t, at).astype(jnp.bfloat16)
            return carry

        lax.fori_loop(0, width // chunk, body, 0)
        core_copy(y, t).start()

    order = []
    for dist in range(n_tp - 1, -1, -1):
        for side in (1, -1) if dist else (1,):
            t = tp + side * dist
            order.append((jnp.logical_and(t >= 0, t < n_tp), t, side, dist))

    def y_copy_b(part, t):
        rows = rows_of[part]
        return remote(work.at[yo, t, rows], yb.at[t, rows], ysend.at[part, t], yrecv.at[part, t],
                      (grp, y_other, tp))

    def y_copy_a():
        return remote(work.at[yo, tp, rows_a], ya, ysend.at[0, 0], yrecv.at[0, 0], (grp, y_other, tp))

    def local(y, t):
        s = y * 2 + core
        core_copy(y, t).wait_recv()

        def body(i, carry):
            at = pl.ds(pl.multiple_of(i * chunk, chunk), chunk)
            both = combined(s, t, at) + from_core[y, t, :, at].astype(jnp.float32)
            work[y, t, :, at] = both.astype(jnp.bfloat16)
            return carry

        lax.fori_loop(0, width // chunk, body, 0)

    def z_ends(part, y, t, slot):
        rows = rows_of[part]
        if part:
            return work.at[y, t, rows], zb.at[slot, rows], bsend.at[part, t], brecv.at[part, slot]
        return work.at[y, t, rows], za.at[y, slot], asend.at[y, t], arecv.at[y, slot]

    def z_copy(part, y, t, side):
        if side == 1:
            slot, target = t, ups
        else:
            slot, target = jnp.where(t == tp - 1, n_tp, t), downs
        return remote(*z_ends(part, y, t, slot), target)

    def take_z(part, y, t, slot):
        remote(*z_ends(part, y, t, slot), ups).wait_recv()
        dst, src = z_ends(part, y, t, slot)[:2]
        add_into(dst, src)

    def z_step(part, y, t, side):
        inner = tp > 0 if side == 1 else tp + 1 < n_tp
        pl.when(inner)(lambda: take_z(part, y, t, t))
        z_copy(part, y, t, side).start()

    def z_end(part, y):
        pl.when(down_ok)(lambda: take_z(part, y, tp, tp))
        pl.when(up_ok)(lambda: take_z(part, y, tp, n_tp))

    for y in (yo, yy):
        for ok, t, side, dist in order:
            pl.when(ok)(functools.partial(combine_away, y, t))
        if y is yo:
            for ok, t, side, dist in order:
                @pl.when(ok)
                def _(t=t):
                    local(yo, t)
                    y_copy_b(1, t).start()
                    y_copy_b(2, t).start()
    for ok, t, side, dist in order:
        @pl.when(ok)
        def _(t=t, side=side, dist=dist):
            local(yy, t)
            if dist:
                z_step(0, yo, t, side)
                z_step(0, yy, t, side)
            for part in (1, 2):
                y_copy_b(part, t).wait_recv()
                add_into(work.at[yy, t, rows_of[part]], yb.at[t, rows_of[part]])
                if dist:
                    z_step(part, yy, t, side)
    z_end(0, yo)
    y_copy_a().start()
    z_end(0, yy)
    z_end(1, yy)
    z_end(2, yy)
    y_copy_a().wait_recv()
    add_into(work.at[yy, tp, rows_a], ya)
    last = pltpu.make_async_copy(work.at[yy, tp], out_ref, own.at[0, 0])
    last.start()
    last.wait()
    y_copy_a().wait_send()
    for ok, t, side, dist in order:
        @pl.when(ok)
        def _(t=t, side=side, dist=dist):
            core_copy(yo, t).wait_send()
            core_copy(yy, t).wait_send()
            y_copy_b(1, t).wait_send()
            y_copy_b(2, t).wait_send()
            if dist:
                z_copy(0, yo, t, side).wait_send()
                z_copy(0, yy, t, side).wait_send()
                z_copy(1, yy, t, side).wait_send()
                z_copy(2, yy, t, side).wait_send()


def add_into(dst, src):
    rows = dst.shape[0]
    strip = 16

    def body(i, carry):
        at = pl.ds(pl.multiple_of(i * strip, strip), strip)
        dst[at] = (dst[at].astype(jnp.float32) + src[at].astype(jnp.float32)).astype(dst.dtype)
        return carry

    lax.fori_loop(0, rows // strip, body, 0)


def dense_experts(normed, routes, route_weight, w_gate, w_up, w_down):
    n_sp, n_tp = lax.axis_size("sp"), lax.axis_size("tp")
    tok, width = normed.shape
    local_experts, _, hidden = w_gate.shape
    n_experts = local_experts * n_sp
    flat_route = routes.reshape(-1)
    onehot = (flat_route[:, None] == lax.iota(jnp.int32, n_experts)[None, :]).astype(jnp.int32)
    rank = jnp.sum((jnp.cumsum(onehot, axis=0) - onehot) * onehot, axis=1).reshape(tok, TOP)
    place = (routes * SLOT + rank).astype(jnp.float32)
    meta = jnp.concatenate([place, route_weight, jnp.zeros((tok, 8 - 2 * TOP), jnp.float32)], axis=1).T
    cuts = ((0, Y_FIRST), (Y_FIRST, Z_PART), (Y_FIRST + Z_PART, tok - Y_FIRST - Z_PART))
    an = cuts[0][1]
    vmem, hbm = pl.BlockSpec(memory_space=pltpu.VMEM), pl.BlockSpec(memory_space=pl.ANY)
    kind = normed.dtype
    slots, buffers = local_experts * SLOT, min(4, local_experts)
    dma = pltpu.SemaphoreType.DMA
    mixed = pl.pallas_call(
        functools.partial(layer_kernel, n_tp, cuts),
        out_shape=jax.ShapeDtypeStruct((tok, width), kind),
        in_specs=[vmem, vmem, hbm, hbm, hbm],
        out_specs=vmem,
        scratch_shapes=[
            pltpu.VMEM((4, n_tp, tok, width), kind),
            pltpu.VMEM((4, n_tp) + meta.shape, jnp.float32),
            pltpu.VMEM((4, n_tp, slots, tok), kind),
            pltpu.VMEM((local_experts, 4 * n_tp * SLOT, 128), jnp.float32),
            pltpu.VMEM((local_experts, 4 * n_tp * SLOT, width), kind),
            pltpu.VMEM((buffers, width, hidden), kind),
            pltpu.VMEM((buffers, width, hidden), kind),
            pltpu.VMEM((buffers, hidden, width), kind),
            pltpu.VMEM((2, n_tp, tok, width), kind),
            pltpu.VMEM((2, n_tp, tok, width), kind),
            pltpu.VMEM((2, n_tp + 1, an, width), kind),
            pltpu.VMEM((n_tp + 1, tok, width), kind),
            pltpu.VMEM((an, width), kind),
            pltpu.VMEM((n_tp, tok, width), kind),
            dma((4, n_tp, 3, 4)),
            dma((4, n_tp, 3)),
            dma((4 * n_tp - 1,)),
            dma((4 * n_tp - 1,)),
            dma((3, buffers)),
            dma((2, n_tp)),
            dma((2, n_tp)),
            dma((2, n_tp)),
            dma((2, n_tp + 1)),
            dma((3, n_tp)),
            dma((3, n_tp + 1)),
            dma((3, n_tp)),
            dma((3, n_tp)),
            dma((2, max(2, n_tp))),
        ],
        compiler_params=pltpu.CompilerParams(
            collective_id=0, has_side_effects=True, vmem_limit_bytes=56 * 2**20
        ),
        name="routed_experts",
    )(normed, meta, w_gate, w_up, w_down)
    return mixed.astype(jnp.float32)


def per_device(
    resid_in,
    pool_input,
    pool_weight,
    pool_scale,
    out_weight,
    mix_gain,
    ffn_gain,
    w_gate,
    w_up,
    w_down,
    routes,
    route_weight,
    post_gain,
):
    n_sp = lax.axis_size("sp")
    n_tp = lax.axis_size("tp")
    seg_rows, channels = pool_input.shape
    if n_sp == 4 and n_tp == GROUPS and channels == GROUP_DIM and seg_rows == n_tp * 128:
        pooled = mixed_tokens(pool_input, pool_weight, pool_scale, n_tp)
    else:
        pooled = routed_pool(pool_input, pool_weight, pool_scale)
    tok_rows = pooled.shape[0]
    mix_out = jnp.dot(pooled, out_weight, preferred_element_type=jnp.float32)
    residual = (resid_in.astype(jnp.float32) + rms_scale(mix_out, mix_gain)).astype(jnp.bfloat16)
    normed = rms_scale(residual.astype(jnp.float32), ffn_gain).astype(jnp.bfloat16)
    width = normed.shape[1]
    if n_sp == 4 and n_tp <= 4 and tok_rows == 128 and w_gate.shape[2] <= 256 and w_gate.shape[0] <= 8 and tok_rows * width <= 128 * 2048:
        expert_mix = dense_experts(normed, routes, route_weight, w_gate, w_up, w_down)
        return (residual.astype(jnp.float32) + rms_scale(expert_mix, post_gain)).astype(jnp.bfloat16)
    local_experts = w_gate.shape[0]
    n_experts = local_experts * n_sp
    slot_total = n_experts * CAP
    flat_route = routes.reshape(-1)
    onehot = (flat_route[:, None] == lax.iota(jnp.int32, n_experts)[None, :]).astype(jnp.int32)
    slot_rank = jnp.sum((jnp.cumsum(onehot, axis=0) - onehot) * onehot, axis=1)
    slot_index = flat_route * CAP + slot_rank
    picker = slot_index[:, None] == lax.iota(jnp.int32, slot_total)[None, :]
    picker_rows = picker.astype(jnp.bfloat16)
    token_pick = jnp.sum(
        picker.reshape(tok_rows, TOP, slot_total).astype(jnp.float32), axis=1
    ).astype(jnp.bfloat16)
    buffer = lax.dot_general(
        token_pick, normed, (((0,), (0,)), ((), ())), preferred_element_type=jnp.float32
    )
    outgoing = buffer.astype(jnp.bfloat16).reshape(n_sp, local_experts * CAP, width)
    at_owner = lax.all_to_all(outgoing, "sp", split_axis=0, concat_axis=0, tiled=True)
    arrived = lax.all_gather(at_owner[:, None], "tp", axis=1, tiled=True)
    arrived = arrived.reshape(n_sp, n_tp, local_experts, CAP, width)
    gate_pre = jnp.einsum("sklcd,ldf->sklcf", arrived, w_gate, preferred_element_type=jnp.float32)
    upward = jnp.einsum("sklcd,ldf->sklcf", arrived, w_up, preferred_element_type=jnp.float32)
    activated = clamped_unit(gate_pre, upward).astype(jnp.bfloat16)
    terms = jnp.einsum("sklcf,lfd->kslcd", activated, w_down, preferred_element_type=jnp.float32)
    summed = lax.psum_scatter(
        terms.reshape(1 * lax.axis_size("tp"), n_sp, local_experts * CAP, width).astype(
            jnp.bfloat16
        ),
        "tp",
        scatter_dimension=0,
        tiled=True,
    ).astype(jnp.float32)
    results = summed[0].astype(jnp.bfloat16)
    returned = lax.all_to_all(results, "sp", split_axis=0, concat_axis=0, tiled=True).reshape(
        slot_total, width
    )
    gathered = jnp.dot(picker_rows, returned, preferred_element_type=jnp.float32)
    expert_mix = jnp.sum(gathered.reshape(tok_rows, TOP, width) * route_weight[:, :, None], axis=1)
    return (residual.astype(jnp.float32) + rms_scale(expert_mix, post_gain)).astype(jnp.bfloat16)


def solution(mesh):
    in_specs = (
        P(("grp", "sp", "tp"), None),
        P(("grp", "sp"), "tp"),
        P(),
        P(),
        P(),
        P(),
        P(),
        P("sp", None, "tp"),
        P("sp", None, "tp"),
        P("sp", "tp", None),
        P(("grp", "sp", "tp"), None),
        P(("grp", "sp", "tp"), None),
        P(),
    )
    out_specs = P(("grp", "sp", "tp"), None)
    return jax.shard_map(
        per_device, mesh=mesh, in_specs=in_specs, out_specs=out_specs, check_vma=False
    )
```

profile of v0, /device:TPU:0, one launch (start us, length us, event | category | flops | bytes accessed | tf_op | source)
XLA Modules:
  0.0 146.3 jit_solution(9055374887555692229)
XLA Ops:
  0.0 14.2 %pool_exchange.1 = bf16[4,144,256]{2,1,0:T(8,128)(2,1)} custom-call(bf16[512,256]{1,0:T(8,128)(2,1)} %pool_ref.1), custom_call_target="tpu_custom_call" | custom-call | tf_op jit(solution)/shard_map/pool_exchange/pallas_call | solution.py:131
  14.2 1.0 slice_convert_fusion.3
  15.2 0.0 copy-start
  15.2 0.9 fusion.74
  16.1 1.3 fusion
  17.4 1.1 fusion.1
  18.6 1.2 fusion.2
  19.7 1.3 fusion.3
  21.0 0.8 multiply_reduce_fusion
  21.9 0.4 fusion.6
  22.3 1.0 fusion.8.row_ref
  23.3 0.1 copy.14
  23.4 0.1 eq.29
  23.5 0.6 reduce-window.6
  24.1 0.2 slice_reduce_fusion
  24.4 0.1 eq.25
  24.5 0.1 fusion.71
  24.6 0.1 reshape.112
  24.8 0.1 copy.17
  24.8 0.1 pad.2.clone
  24.9 0.7 maximum_bitcast_fusion.meta_ref
  25.6 117.3 %routed_experts.1 = bf16[128,2048]{1,0:T(8,128)(2,1)} custom-call(bf16[128,2048]{1,0:T(8,128)(2,1)} %fusion.8.row_ref, f32[8,128]{1,0:T(8,128)} %maximum_bitcast_fusion.meta_ref, bf16[8,2048,256]{2,1,0:T(8,128)(2,1)} %wg_ref.1, bf16[8,2048,256]{2,1,0:T(8,128)(2,1)} %wu_ref.1, bf16[8,256,2048]{2,1,0:T(8,128)(2,1)} %wd_ref.1), custom_call_target="tpu_custom_call" | custom-call | tf_op jit(solution)/shard_map/routed_experts/pallas_call | solution.py:533
  142.9 1.2 fusion.4
  144.2 2.1 %fusion.9 = bf16[128,2048]{1,0:T(8,128)(2,1)} fusion(bf16[128,2048]{1,0:T(8,128)(2,1)} %routed_experts.1, bf16[128,2048]{1,0:T(8,128)(2,1)S(1)} %get-tuple-element.6, f32[2048]{0:T(1024)S(1)} %copy-done.4, f32[128]{0:T(128)S(1)} %add_rsqrt_fusion), kind=kLoop, calls=%fused_computation.18 | loop fusion | flops 1572864 | bytes 1581568 | tf_op jit(solution)/shard_map/convert_element_type | solution.py:605
  (23 shorter events, 0.1 us)
Async XLA Ops:
  15.2 5.8 %copy-start = (bf16[1024,2048]{1,0:T(8,128)(2,1)S(1)}, bf16[1024,2048]{1,0:T(8,128)(2,1)}, u32[]{:S(2)}) copy-start(bf16[1024,2048]{1,0:T(8,128)(2,1)} %param.17) | copy-start | bytes 12582916
  19.7 2.2 %copy-start.1 = (bf16[128,2048]{1,0:T(8,128)(2,1)S(1)}, bf16[128,2048]{1,0:T(8,128)(2,1)}, u32[]{:S(2)}) copy-start(bf16[128,2048]{1,0:T(8,128)(2,1)} %param.13) | copy-start | bytes 1572868
  19.7 2.2 %copy-start.2 = (f32[2048]{0:T(1024)S(1)}, f32[2048]{0:T(1024)}, u32[]{:S(2)}) copy-start(f32[2048]{0:T(1024)} %param.18) | copy-start | bytes 24580
  21.0 1.3 copy-start.3
  21.0 2.3 %copy-start.5 = (s32[128,2]{0,1:T(2,128)S(1)}, s32[128,2]{0,1:T(2,128)}, u32[]{:S(2)}) copy-start(s32[128,2]{0,1:T(2,128)} %param.23) | copy-start | bytes 3076
  21.0 3.9 %copy-start.6 = (f32[128,2]{0,1:T(2,128)S(1)}, f32[128,2]{0,1:T(2,128)}, u32[]{:S(2)}) copy-start(f32[128,2]{0,1:T(2,128)} %param.24) | copy-start | bytes 3076
  25.6 118.6 %copy-start.4 = (f32[2048]{0:T(1024)S(1)}, f32[2048]{0:T(1024)}, u32[]{:S(2)}) copy-start(f32[2048]{0:T(1024)} %param.25) | copy-start | bytes 24580
where the time goes:
time: 147 us; the launch traced here: 146 us
  Pallas kernels  131 us (89%)
  other arithmetic  7.16 us (5%)
  matrix products  5.69 us (4%)
  local copies, waits for them, and re-layouts  1.81 us (1%)
    pallas_call x1, Pallas kernels, dense_experts(): pl.pallas_call(functools.partial(layer_kernel, n_tp, cuts), out_shape=jax...  117 us
    pallas_call x1, Pallas kernels, mixed_tokens(): pl.pallas_call(functools.partial(exchange_kernel, n_tp), out_shape=jax.Sh...  14.2 us
    dot_general x4, matrix products, mixed_tokens(): jnp.dot(mixed, pool_weight[group], preferred_element_type=jnp.float32)  4.87 us

commit v1 on v0

--- a/solution.py
+++ b/solution.py
@@ -45,112 +45,6 @@
 
 def coords():
     return lax.axis_index("grp"), lax.axis_index("sp"), lax.axis_index("tp")
-
-
-def exchange_kernel(n_tp, pool_ref, out_ref, send, recv, hsend, hrecv, own):
-    grp, sp, tp = coords()
-    seg_rows = pool_ref.shape[0]
-    tok, reach = seg_rows // n_tp, SLOT
-    first = tp == 0
-    others = [(a, b) for a in range(4) for b in range(n_tp) if (a, b) != (0, 0)]
-    barrier = pltpu.get_barrier_semaphore()
-    for by in others:
-        target = (grp, (sp + by[0]) % 4, (tp + by[1]) % n_tp)
-        pl.semaphore_signal(barrier, inc=1, device_id=target, device_id_type=MESH)
-
-    def ends(to, whole, chan):
-        if whole:
-            at = pl.multiple_of(to * tok - reach, reach)
-            return pool_ref.at[pl.ds(at, tok + reach)], out_ref.at[chan]
-        return pool_ref.at[pl.ds(0, tok)], out_ref.at[chan, pl.ds(reach, tok)]
-
-    def main(by, whole):
-        to = (tp + by) % n_tp
-        src, dst = ends(to, whole, tp)
-        return pltpu.make_async_remote_copy(
-            src_ref=src, dst_ref=dst, send_sem=send.at[by], recv_sem=recv.at[tp],
-            device_id=(grp, sp, to), device_id_type=MESH)
-
-    def arrival(by, whole):
-        chan = (tp + by) % n_tp
-        src, dst = ends(1 if whole else 0, whole, chan)
-        return pltpu.make_async_remote_copy(
-            src_ref=src, dst_ref=dst, send_sem=send.at[by], recv_sem=recv.at[chan],
-            device_id=(grp, sp, chan), device_id_type=MESH)
-
-    def halo(chan):
-        return pltpu.make_async_remote_copy(
-            src_ref=pool_ref.at[pl.ds(seg_rows - reach, reach)],
-            dst_ref=out_ref.at[chan, pl.ds(0, reach)],
-            send_sem=hsend.at[0], recv_sem=hrecv.at[chan],
-            device_id=(grp, sp + 1, 0), device_id_type=MESH)
-
-    def kept(whole):
-        src, dst = ends(tp, whole, tp)
-        return pltpu.make_async_copy(src, dst, own.at[0])
-
-    pl.semaphore_wait(barrier, len(others))
-    rest = jnp.logical_not(first)
-    has_next = sp + 1 < 4
-    pl.when(has_next)(lambda: halo(tp).start())
-    for by in range(1, n_tp):
-        to_first = (tp + by) % n_tp == 0
-        pl.when(to_first)(lambda by=by: main(by, False).start())
-        pl.when(jnp.logical_not(to_first))(lambda by=by: main(by, True).start())
-    pl.when(first)(lambda: kept(False).start())
-    pl.when(rest)(lambda: kept(True).start())
-
-    @pl.when(jnp.logical_and(first, sp == 0))
-    def _():
-        for chan in range(n_tp):
-            out_ref[chan, pl.ds(0, reach)] = jnp.zeros((reach, out_ref.shape[2]), out_ref.dtype)
-
-    pl.when(first)(lambda: kept(False).wait())
-    pl.when(rest)(lambda: kept(True).wait())
-    for by in range(1, n_tp):
-        pl.when(first)(lambda by=by: arrival(by, False).wait_recv())
-        pl.when(rest)(lambda by=by: arrival(by, True).wait_recv())
-
-    @pl.when(jnp.logical_and(first, sp > 0))
-    def _():
-        for chan in range(n_tp):
-            halo(chan).wait_recv()
-
-    pl.when(has_next)(lambda: halo(tp).wait_send())
-    for by in range(1, n_tp):
-        to_first = (tp + by) % n_tp == 0
-        pl.when(to_first)(lambda by=by: main(by, False).wait_send())
-        pl.when(jnp.logical_not(to_first))(lambda by=by: main(by, True).wait_send())
-
-
-def mixed_tokens(pool_input, pool_weight, pool_scale, n_tp):
-    seg_rows, channels = pool_input.shape
-    tok = seg_rows // n_tp
-    vmem = pl.BlockSpec(memory_space=pltpu.VMEM)
-    dma = pltpu.SemaphoreType.DMA
-    rows = pl.pallas_call(
-        functools.partial(exchange_kernel, n_tp),
-        out_shape=jax.ShapeDtypeStruct((n_tp, tok + SLOT, channels), pool_input.dtype),
-        in_specs=[vmem],
-        out_specs=vmem,
-        scratch_shapes=[dma((n_tp,)), dma((n_tp,)), dma((1,)), dma((n_tp,)), dma((1,))],
-        compiler_params=pltpu.CompilerParams(collective_id=1, has_side_effects=True),
-        name="pool_exchange",
-    )(pool_input)
-    start = (lax.axis_index("sp") * n_tp + lax.axis_index("tp")) * tok
-    count = start + lax.broadcasted_iota(jnp.int32, (tok, 1), 0) + 1
-    pooled = []
-    for group, window in enumerate(pool_windows):
-        held = rows[group].astype(jnp.float32)
-        total = held[SLOT:]
-        for offset in range(1, window):
-            total = total + held[SLOT - offset : SLOT - offset + tok]
-        divisor = jnp.minimum(count, window).astype(jnp.float32)
-        mixed = (total / divisor - held[SLOT:]).astype(jnp.bfloat16)
-        product = jnp.dot(mixed, pool_weight[group], preferred_element_type=jnp.float32)
-        scale = pool_scale[group * GROUP_DIM : (group + 1) * GROUP_DIM]
-        pooled.append((product * scale).astype(jnp.bfloat16))
-    return jnp.concatenate(pooled, axis=1)
 
 
 def routed_pool(pool_input, pool_weight, pool_scale):
@@ -187,9 +81,12 @@
     return pooled
 
 
-def layer_kernel(n_tp, cuts, row_ref, meta_ref, wg_ref, wu_ref, wd_ref, out_ref,
+def layer_kernel(n_tp, cuts, pool_ref, pw_ref, scale_ref, ow_ref, resid_ref, mgain_ref, fgain_ref,
+                 pgain_ref, routes_ref, rweight_ref, wg_ref, wu_ref, wd_ref, out_ref,
+                 pool, rows_in, pw, ow, residual, pooled, mix,
                  every, metas, picks, weights, held, wg, wu, wd,
                  work, from_core, za, zb, ya, yb,
+                 psend, precv, hsend, hrecv, fsem,
                  send, recv, msend, mrecv, wsem,
                  csend, crecv, asend, arecv, bsend, brecv, ysend, yrecv, own):
     grp, sp, tp = coords()
@@ -197,7 +94,7 @@
     yo = 1 - yy
     y_other = yo * 2 + core
     c_other = yy * 2 + (1 - core)
-    tok, width = row_ref.shape
+    tok, width = residual.shape
     local_experts, buffers = wg_ref.shape[0], wg.shape[0]
     slots = local_experts * SLOT
     chunk = min(1024, width)
@@ -208,24 +105,123 @@
         return [pltpu.make_async_copy(w.at[e], buf.at[at], wsem.at[i, at])
                 for i, (w, buf) in enumerate(((wg_ref, wg), (wu_ref, wu), (wd_ref, wd)))]
 
-    own_copy = pltpu.make_async_copy(row_ref, every.at[sp, tp], own.at[0, 0])
-    own_copy.start()
-    own_meta = pltpu.make_async_copy(meta_ref, metas.at[sp, tp], own.at[0, 1])
-    own_meta.start()
+    loads = [pltpu.make_async_copy(a, b, fsem.at[i]) for i, (a, b) in enumerate(
+        ((pool_ref, pool), (pw_ref, pw), (resid_ref, residual), (ow_ref, ow)))]
+    for c in loads:
+        c.start()
     barrier = pltpu.get_barrier_semaphore()
     for by in others:
         target = (grp, (sp + by[0]) % 4, (tp + by[1]) % n_tp)
         pl.semaphore_signal(barrier, inc=1, device_id=target, device_id_type=MESH)
+    metas[sp, tp] = token_meta(routes_ref, rweight_ref, local_experts * 4)
+    loads[0].wait()
     pl.semaphore_wait(barrier, len(others))
 
     def meta_copy(number, by):
         return pltpu.make_async_remote_copy(
-            src_ref=meta_ref, dst_ref=metas.at[sp, tp],
+            src_ref=metas.at[sp, tp], dst_ref=metas.at[sp, tp],
             send_sem=msend.at[number], recv_sem=mrecv.at[number],
             device_id=(grp, (sp + by[0]) % 4, (tp + by[1]) % n_tp), device_id_type=MESH)
 
-    own_copy.wait()
-    own_meta.wait()
+    seg_rows, reach = pool.shape[0], SLOT
+    first = tp == 0
+    rest = tp > 0
+    has_next = sp + 1 < 4
+
+    def ends(to, whole, chan):
+        if whole:
+            at = pl.multiple_of(to * tok - reach, reach)
+            return pool.at[pl.ds(at, tok + reach)], rows_in.at[chan]
+        return pool.at[pl.ds(0, tok)], rows_in.at[chan, pl.ds(reach, tok)]
+
+    def spread(by, whole):
+        to = (tp + by) % n_tp
+        src, dst = ends(to, whole, tp)
+        return pltpu.make_async_remote_copy(
+            src_ref=src, dst_ref=dst, send_sem=psend.at[by], recv_sem=precv.at[tp],
+            device_id=(grp, sp, to), device_id_type=MESH)
+
+    def landed(chan, whole):
+        src, dst = ends(1 if whole else 0, whole, chan)
+        return pltpu.make_async_remote_copy(
+            src_ref=src, dst_ref=dst, send_sem=psend.at[0], recv_sem=precv.at[chan],
+            device_id=(grp, sp, tp), device_id_type=MESH)
+
+    def halo(chan):
+        return pltpu.make_async_remote_copy(
+            src_ref=pool.at[pl.ds(seg_rows - reach, reach)],
+            dst_ref=rows_in.at[chan, pl.ds(0, reach)],
+            send_sem=hsend.at[0], recv_sem=hrecv.at[chan],
+            device_id=(grp, sp + 1, 0), device_id_type=MESH)
+
+    def kept(whole):
+        src, dst = ends(tp, whole, tp)
+        return pltpu.make_async_copy(src, dst, own.at[0, 1])
+
+    pl.when(has_next)(lambda: halo(tp).start())
+    for by in range(1, n_tp):
+        to_first = (tp + by) % n_tp == 0
+        pl.when(to_first)(lambda by=by: spread(by, False).start())
+        pl.when(jnp.logical_not(to_first))(lambda by=by: spread(by, True).start())
+    pl.when(first)(lambda: kept(False).start())
+    pl.when(rest)(lambda: kept(True).start())
+    for number, by in enumerate(others):
+        meta_copy(number, by).start()
+    for e in range(min(buffers, local_experts)):
+        for c in weight_copies(e):
+            c.start()
+
+    @pl.when(jnp.logical_and(first, sp == 0))
+    def _():
+        for chan in range(n_tp):
+            rows_in[chan, pl.ds(0, reach)] = jnp.zeros((reach, rows_in.shape[2]), rows_in.dtype)
+
+    loads[1].wait()
+    start = (sp * n_tp + tp) * tok
+    for group, window in enumerate(pool_windows):
+        mine = tp == group
+        if group:
+            pl.when(mine)(lambda: kept(True).wait())
+            pl.when(first)(lambda g=group: landed(g, False).wait_recv())
+            pl.when(jnp.logical_and(rest, tp != group))(lambda g=group: landed(g, True).wait_recv())
+        else:
+            pl.when(mine)(lambda: kept(False).wait())
+            pl.when(rest)(lambda: landed(0, True).wait_recv())
+        pl.when(jnp.logical_and(first, sp > 0))(lambda g=group: halo(g).wait_recv())
+        values = rows_in[group].astype(jnp.float32)
+        total = values
+        span = 1
+        while span < window:
+            total = total + jnp.concatenate([total[:span], total[:-span]], axis=0)
+            span *= 2
+        count = start + lax.broadcasted_iota(jnp.int32, (tok, values.shape[1]), 0) + 1
+        divisor = jnp.minimum(count, window).astype(jnp.float32)
+        mixed = (total[reach:] / divisor - values[reach:]).astype(jnp.bfloat16)
+        product = jnp.dot(mixed, pw[group], preferred_element_type=jnp.float32)
+        cols = slice(group * GROUP_DIM, (group + 1) * GROUP_DIM)
+        pooled[:, cols] = (product * scale_ref[:, cols]).astype(jnp.bfloat16)
+    loads[3].wait()
+
+    def project(i, carry):
+        at = pl.ds(pl.multiple_of(i * 512, 512), 512)
+        mix[:, at] = jnp.dot(pooled[...], ow[:, at], preferred_element_type=jnp.float32)
+        return carry
+
+    lax.fori_loop(0, width // 512, project, 0)
+    loads[2].wait()
+
+    def norm_rows(part):
+        begin, count = cuts[part]
+
+        def body(i, carry):
+            at = pl.ds(pl.multiple_of(begin + i * SLOT, SLOT), SLOT)
+            after = residual[at].astype(jnp.float32) + rms_scale(mix[at], mgain_ref[...])
+            after = after.astype(jnp.bfloat16)
+            residual[at] = after
+            every[sp, tp, at] = rms_scale(after.astype(jnp.float32), fgain_ref[...]).astype(jnp.bfloat16)
+            return carry
+
+        lax.fori_loop(0, count // SLOT, body, 0)
 
     def copy(s, t, part, way):
         target = [(grp, sp, tp + 1), (grp, sp, tp - 1), (grp, y_other, tp), (grp, c_other, tp)][way]
@@ -279,10 +275,10 @@
         lax.fori_loop(0, width // chunk, body, 0)
 
     yes = tp >= 0
-    for number, by in enumerate(others):
-        meta_copy(number, by).start()
+    norm_rows(0)
     push(yes, sp, tp, 0, 2)
     for part in (1, 2):
+        norm_rows(part)
         push(yes, sp, tp, part, 0)
         push(yes, sp, tp, part, 1)
         push(yes, sp, tp, part, 2)
@@ -290,16 +286,13 @@
     push(yes, sp, tp, 0, 1)
     for part in (0, 1, 2):
         push(yes, sp, tp, part, 3)
-    for e in range(min(buffers, local_experts)):
-        for c in weight_copies(e):
-            c.start()
     arrived(y_other, tp, 0)
     push(yes, y_other, tp, 0, 0)
     push(yes, y_other, tp, 0, 1)
     push(yes, y_other, tp, 0, 3)
-    select(sp, tp)
     for number, by in enumerate(others):
         meta_copy(number, by).wait()
+    select(sp, tp)
 
     def sides(dist):
         if dist == 0:
@@ -484,9 +477,18 @@
     z_end(2, yy)
     y_copy_a().wait_recv()
     add_into(work.at[yy, tp, rows_a], ya)
-    last = pltpu.make_async_copy(work.at[yy, tp], out_ref, own.at[0, 0])
-    last.start()
-    last.wait()
+    def finish(i, carry):
+        at = pl.ds(pl.multiple_of(i * SLOT, SLOT), SLOT)
+        total = work[yy, tp, at].astype(jnp.float32)
+        out_ref[at] = (residual[at].astype(jnp.float32) + rms_scale(total, pgain_ref[...])).astype(out_ref.dtype)
+        return carry
+
+    lax.fori_loop(0, tok // SLOT, finish, 0)
+    pl.when(has_next)(lambda: halo(tp).wait_send())
+    for by in range(1, n_tp):
+        to_first = (tp + by) % n_tp == 0
+        pl.when(to_first)(lambda by=by: spread(by, False).wait_send())
+        pl.when(jnp.logical_not(to_first))(lambda by=by: spread(by, True).wait_send())
     y_copy_a().wait_send()
     for ok, t, side, dist in order:
         @pl.when(ok)
@@ -502,6 +504,24 @@
                 z_copy(2, yy, t, side).wait_send()
 
 
+def token_meta(routes_ref, rweight_ref, n_experts):
+    tok = routes_ref.shape[1]
+    expert = lax.broadcasted_iota(jnp.int32, (n_experts, tok), 0)
+    hits = [jnp.where(expert == routes_ref[k : k + 1], 1.0, 0.0) for k in range(TOP)]
+    earlier = (lax.broadcasted_iota(jnp.int32, (tok, tok), 0)
+               < lax.broadcasted_iota(jnp.int32, (tok, tok), 1))
+    earlier = jnp.where(earlier, 1.0, 0.0).astype(jnp.bfloat16)
+    before = jnp.dot(sum(hits).astype(jnp.bfloat16), earlier, preferred_element_type=jnp.float32)
+    line = lax.broadcasted_iota(jnp.int32, (8, tok), 0)
+    meta = jnp.zeros((8, tok), jnp.float32)
+    for k in range(TOP):
+        rank = jnp.sum(hits[k] * before, axis=0, keepdims=True)
+        place = routes_ref[k : k + 1].astype(jnp.float32) * SLOT + rank
+        meta = jnp.where(line == k, place, meta)
+        meta = jnp.where(line == TOP + k, rweight_ref[k : k + 1], meta)
+    return meta
+
+
 def add_into(dst, src):
     rows = dst.shape[0]
     strip = 16
@@ -514,30 +534,33 @@
     lax.fori_loop(0, rows // strip, body, 0)
 
 
-def dense_experts(normed, routes, route_weight, w_gate, w_up, w_down):
-    n_sp, n_tp = lax.axis_size("sp"), lax.axis_size("tp")
-    tok, width = normed.shape
+def fused_layer(resid_in, pool_input, pool_weight, pool_scale, out_weight, mix_gain, ffn_gain,
+                w_gate, w_up, w_down, routes, route_weight, post_gain):
+    n_tp = lax.axis_size("tp")
+    tok, width = resid_in.shape
     local_experts, _, hidden = w_gate.shape
-    n_experts = local_experts * n_sp
-    flat_route = routes.reshape(-1)
-    onehot = (flat_route[:, None] == lax.iota(jnp.int32, n_experts)[None, :]).astype(jnp.int32)
-    rank = jnp.sum((jnp.cumsum(onehot, axis=0) - onehot) * onehot, axis=1).reshape(tok, TOP)
-    place = (routes * SLOT + rank).astype(jnp.float32)
-    meta = jnp.concatenate([place, route_weight, jnp.zeros((tok, 8 - 2 * TOP), jnp.float32)], axis=1).T
     cuts = ((0, Y_FIRST), (Y_FIRST, Z_PART), (Y_FIRST + Z_PART, tok - Y_FIRST - Z_PART))
     an = cuts[0][1]
     vmem, hbm = pl.BlockSpec(memory_space=pltpu.VMEM), pl.BlockSpec(memory_space=pl.ANY)
-    kind = normed.dtype
+    kind = resid_in.dtype
     slots, buffers = local_experts * SLOT, min(4, local_experts)
+    channels = pool_input.shape[1]
     dma = pltpu.SemaphoreType.DMA
-    mixed = pl.pallas_call(
+    return pl.pallas_call(
         functools.partial(layer_kernel, n_tp, cuts),
         out_shape=jax.ShapeDtypeStruct((tok, width), kind),
-        in_specs=[vmem, vmem, hbm, hbm, hbm],
+        in_specs=[hbm, hbm, vmem, hbm, hbm, vmem, vmem, vmem, vmem, vmem, hbm, hbm, hbm],
         out_specs=vmem,
         scratch_shapes=[
+            pltpu.VMEM(pool_input.shape, kind),
+            pltpu.VMEM((n_tp, tok + SLOT, channels), kind),
+            pltpu.VMEM(pool_weight.shape, kind),
+            pltpu.VMEM(out_weight.shape, kind),
+            pltpu.VMEM((tok, width), kind),
+            pltpu.VMEM((tok, n_tp * channels), kind),
+            pltpu.VMEM((tok, width), jnp.float32),
             pltpu.VMEM((4, n_tp, tok, width), kind),
-            pltpu.VMEM((4, n_tp) + meta.shape, jnp.float32),
+            pltpu.VMEM((4, n_tp, 8, tok), jnp.float32),
             pltpu.VMEM((4, n_tp, slots, tok), kind),
             pltpu.VMEM((local_experts, 4 * n_tp * SLOT, 128), jnp.float32),
             pltpu.VMEM((local_experts, 4 * n_tp * SLOT, width), kind),
@@ -550,6 +573,11 @@
             pltpu.VMEM((n_tp + 1, tok, width), kind),
             pltpu.VMEM((an, width), kind),
             pltpu.VMEM((n_tp, tok, width), kind),
+            dma((n_tp,)),
+            dma((n_tp,)),
+            dma((1,)),
+            dma((n_tp,)),
+            dma((4,)),
             dma((4, n_tp, 3, 4)),
             dma((4, n_tp, 3)),
             dma((4 * n_tp - 1,)),
@@ -566,11 +594,11 @@
             dma((2, max(2, n_tp))),
         ],
         compiler_params=pltpu.CompilerParams(
-            collective_id=0, has_side_effects=True, vmem_limit_bytes=56 * 2**20
+            collective_id=0, has_side_effects=True, vmem_limit_bytes=58 * 2**20
         ),
-        name="routed_experts",
-    )(normed, meta, w_gate, w_up, w_down)
-    return mixed.astype(jnp.float32)
+        name="fused_layer",
+    )(pool_input, pool_weight, pool_scale[None], out_weight, resid_in, mix_gain[None], ffn_gain[None],
+      post_gain[None], routes.T, route_weight.T, w_gate, w_up, w_down)
 
 
 def per_device(
@@ -591,18 +619,23 @@
     n_sp = lax.axis_size("sp")
     n_tp = lax.axis_size("tp")
     seg_rows, channels = pool_input.shape
-    if n_sp == 4 and n_tp == GROUPS and channels == GROUP_DIM and seg_rows == n_tp * 128:
-        pooled = mixed_tokens(pool_input, pool_weight, pool_scale, n_tp)
-    else:
-        pooled = routed_pool(pool_input, pool_weight, pool_scale)
-    tok_rows = pooled.shape[0]
+    tok_rows, width = resid_in.shape
+    if (
+        n_sp == 4
+        and n_tp == GROUPS
+        and channels == GROUP_DIM
+        and seg_rows == n_tp * 128
+        and tok_rows == 128
+        and w_gate.shape[2] <= 256
+        and w_gate.shape[0] <= 8
+        and width <= 2048
+    ):
+        return fused_layer(resid_in, pool_input, pool_weight, pool_scale, out_weight, mix_gain,
+                           ffn_gain, w_gate, w_up, w_down, routes, route_weight, post_gain)
+    pooled = routed_pool(pool_input, pool_weight, pool_scale)
     mix_out = jnp.dot(pooled, out_weight, preferred_element_type=jnp.float32)
     residual = (resid_in.astype(jnp.float32) + rms_scale(mix_out, mix_gain)).astype(jnp.bfloat16)
     normed = rms_scale(residual.astype(jnp.float32), ffn_gain).astype(jnp.bfloat16)
-    width = normed.shape[1]
-    if n_sp == 4 and n_tp <= 4 and tok_rows == 128 and w_gate.shape[2] <= 256 and w_gate.shape[0] <= 8 and tok_rows * width <= 128 * 2048:
-        expert_mix = dense_experts(normed, routes, route_weight, w_gate, w_up, w_down)
-        return (residual.astype(jnp.float32) + rms_scale(expert_mix, post_gain)).astype(jnp.bfloat16)
     local_experts = w_gate.shape[0]
     n_experts = local_experts * n_sp
     slot_total = n_experts * CAP

time: 147 us -> 130 us (0.88)
  other arithmetic: 7.16 us -> 0 us
  matrix products: 5.69 us -> 0 us
  Pallas kernels: 131 us -> 128 us
    dot_general x5 -> x0, matrix products: 5.69 us -> none  [the longest x4 4.87 us: mixed_tokens(): jnp.dot(mixed, pool_weight[group], preferred_element_type=jnp.float32)]
    convert_element_type x7 -> x0, other arithmetic: 4.14 us -> none  [the longest x1 2.09 us: per_device(): (residual.astype(jnp.float32) + rms_scale(expert_mix, post_gain)).astype(...]
    pallas_call x2 -> x1, Pallas kernels: 131 us -> 128 us  [fused_layer(): pl.pallas_call(functools.partial(layer_kernel, n_tp, cuts), out_shape=jax...]
    unnamed x15 -> x1, local copies, waits for them, and re-layouts: 0.15 us -> 1.88 us
    reduce_sum x3 -> x0, other arithmetic: 1.7 us -> none  [the longest x2 1.6 us: rms_scale(): jnp.mean(values * values, axis=-1, keepdims=True) + norm_eps]
where the time goes in v1:
time: 130 us
  Pallas kernels  128 us (98%)
  local copies, waits for them, and re-layouts  1.88 us (1%)
    pallas_call x1, Pallas kernels, fused_layer(): pl.pallas_call(functools.partial(layer_kernel, n_tp, cuts), out_shape=jax...  128 us

profile of v1, /device:TPU:0, one launch (start us, length us, event | category | flops | bytes accessed | tf_op | source)
XLA Modules:
  0.0 130.0 jit_solution(8622462533673119225)
XLA Ops:
  0.0 128.1 %fused_layer.1 = bf16[128,2048]{1,0:T(8,128)(2,1)} custom-call(bf16[512,256]{1,0:T(8,128)(2,1)} %pool_ref.1, bf16[4,256,256]{2,1,0:T(8,128)(2,1)} %pw_ref.1, f32[1,1024]{1,0:T(1,128)} %bitcast.9, bf16[1024,2048]{1,0:T(8,128)(2,1)} %ow_ref.1, bf16[128,2048]{1,0:T(8,128)(2,1)} %resid_ref.1, f32[1,2048]{1,0:T(1,128)} %bitcast.6, f32[1,2048]{1,0:T(1,128)} %bitcast.7, ...), custom_call_target="tpu_custom_call" | custom-call | tf_op jit(solution)/shard_map/fused_layer/pallas_call | solution.py:549
  128.1 1.9 %copy.15 = bf16[128,2048]{1,0:T(8,128)(2,1)} copy(bf16[128,2048]{1,0:T(8,128)(2,1)} %fused_layer.1) | data formatting | bytes 1048576

commit v2 on v1

--- a/solution.py
+++ b/solution.py
@@ -38,8 +38,38 @@
 
 
 SLOT = 16
-Y_FIRST = 16
-Z_PART = 64
+HALVES = ((16, 16, 32), (16, 32, 16))
+BACK = ((16, 16, 32), (16, 32, 16))
+ORDER = (
+    ("N", 0, 0), ("OZ", 0, 0), ("N", 0, 2), ("OY", 0, 2), ("N", 1, 4), ("OY", 0, 0), ("N", 1, 5),
+    ("N", 0, 1), ("OZ", 0, 1), ("OY", 0, 1), ("OZ", 0, 2), ("F", 0, 1, 0, "own"), ("N", 1, 3),
+    ("OC", 1), ("F", 0, 1, 1, "own"), ("X", 0), ("F", 0, 2, 0, "own"), ("F", 0, 1, 2, "own"),
+    ("F", 0, 2, 1, "own"), ("F", 0, 2, 2, "own"), ("OC", 0), ("F", 0, 1, 0, "yo"),
+    ("F", 0, 3, 1, "own"), ("YS", 0, 0), ("F", 0, 3, 2, "own"), ("OY", 1, 4), ("SA", 0, 0),
+    ("F", 0, 3, 0, "own"), ("CO", 0, 2), ("SA", 1, 0), ("SA", 0, 2), ("OZ", 1, 5),
+    ("F", 0, 2, 0, "yo"), ("YS", 0, 1), ("YS", 0, 2), ("CO", 0, 3), ("OY", 1, 3), ("OZ", 1, 4),
+    ("CO", 0, 0), ("OZ", 1, 3), ("SA", 0, 3), ("FA", 0, 1), ("OY", 1, 5), ("FA", 0, 2),
+    ("SA", 0, 1), ("F", 0, 3, 0, "yo"), ("YS", 0, 3), ("FA", 0, 0), ("F", 1, 1, 5, "own"),
+    ("FA", 0, 3), ("CO", 0, 1), ("E", 0, 0), ("F", 1, 1, 4, "own"), ("E", 0, 1), ("E", 0, 2),
+    ("X", 1), ("F", 1, 2, 5, "own"), ("E", 0, 3), ("E", 0, 4), ("E", 0, 5), ("F", 1, 2, 4, "own"),
+    ("E", 0, 6), ("E", 0, 7), ("F", 1, 1, 3, "yo"), ("AW", 0, "yo", 3), ("AW", 0, "yo", 2),
+    ("F", 1, 1, 3, "own"), ("AW", 0, "yy", 3), ("F", 1, 3, 5, "own"), ("AW", 0, "yy", 1),
+    ("AW", 0, "yo", 1), ("CO", 1, 0), ("AW", 0, "yy", 2), ("F", 1, 3, 4, "own"), ("SY", 0, 3),
+    ("RL", 0, 3), ("AW", 0, "yy", 0), ("F", 1, 2, 3, "yo"), ("SA", 1, 1), ("YS", 1, 0),
+    ("YS", 1, 2), ("SY", 0, 2), ("F", 1, 2, 3, "own"), ("YS", 1, 1), ("RL", 0, 2), ("SY", 0, 1),
+    ("FA", 1, 2), ("SA", 1, 2), ("FA", 1, 1), ("FA", 1, 0), ("F", 1, 3, 3, "yo"), ("YS", 1, 3),
+    ("F", 1, 3, 3, "own"), ("CO", 1, 1), ("RL", 0, 1), ("FA", 1, 3), ("AW", 0, "yo", 0),
+    ("CO", 1, 3), ("RT", 0, 3, 1), ("CO", 1, 2), ("SA", 1, 3), ("E", 1, 0), ("RT", 0, 3, 2),
+    ("E", 1, 1), ("E", 1, 2), ("RT", 0, 2, 1), ("E", 1, 3), ("E", 1, 4), ("RT", 0, 2, 2),
+    ("SY", 0, 0), ("E", 1, 5), ("E", 1, 6), ("E", 1, 7), ("RT", 0, 1, 1), ("AW", 1, "yo", 3),
+    ("AW", 1, "yy", 0), ("RL", 0, 0), ("AW", 1, "yo", 2), ("RT", 0, 1, 2), ("AW", 1, "yy", 3),
+    ("AW", 1, "yy", 2), ("SY", 1, 3), ("AW", 1, "yo", 1), ("RL", 1, 3), ("RH", 0), ("RT", 0, 0, 2),
+    ("RT", 1, 3, 4), ("SY", 1, 2), ("RT", 1, 3, 5), ("AW", 1, "yy", 1), ("RL", 1, 2),
+    ("RT", 0, 0, 1), ("RP", 0, 1), ("SY", 1, 1), ("RP", 0, 2), ("AW", 1, "yo", 0), ("RF", 0),
+    ("RT", 1, 2, 4), ("RT", 1, 2, 5), ("SY", 1, 0), ("RL", 1, 1), ("RT", 1, 1, 4), ("RL", 1, 0),
+    ("RT", 1, 1, 5), ("RH", 1), ("RT", 1, 0, 5), ("RT", 1, 0, 4), ("RP", 1, 4), ("RP", 1, 5),
+    ("RF", 1),
+)
 MESH = pl.DeviceIdType.MESH
 
 
@@ -81,9 +111,9 @@
     return pooled
 
 
-def layer_kernel(n_tp, cuts, pool_ref, pw_ref, scale_ref, ow_ref, resid_ref, mgain_ref, fgain_ref,
+def layer_kernel(n_tp, cuts, rcuts, pool_ref, pw_ref, scale_ref, ow_ref, resid_ref, mgain_ref, fgain_ref,
                  pgain_ref, routes_ref, rweight_ref, wg_ref, wu_ref, wd_ref, out_ref,
-                 pool, rows_in, pw, ow, residual, pooled, mix,
+                 pool, rows_in, pw, residual, pooled, mix,
                  every, metas, picks, weights, held, wg, wu, wd,
                  work, from_core, za, zb, ya, yb,
                  psend, precv, hsend, hrecv, fsem,
@@ -97,7 +127,7 @@
     tok, width = residual.shape
     local_experts, buffers = wg_ref.shape[0], wg.shape[0]
     slots = local_experts * SLOT
-    chunk = min(1024, width)
+    chunk = width
     others = [(a, b) for a in range(4) for b in range(n_tp) if (a, b) != (0, 0)]
 
     def weight_copies(e):
@@ -106,7 +136,10 @@
                 for i, (w, buf) in enumerate(((wg_ref, wg), (wu_ref, wu), (wd_ref, wd)))]
 
     loads = [pltpu.make_async_copy(a, b, fsem.at[i]) for i, (a, b) in enumerate(
-        ((pool_ref, pool), (pw_ref, pw), (resid_ref, residual), (ow_ref, ow)))]
+        ((pool_ref, pool), (pw_ref, pw), (resid_ref, residual)))]
+    blocks = [(y, t) for y in range(2) for t in range(n_tp)]
+    loads += [pltpu.make_async_copy(ow_ref.at[pl.ds(i * tok, tok)], from_core.at[y, t], fsem.at[3 + i])
+              for i, (y, t) in enumerate(blocks)]
     for c in loads:
         c.start()
     barrier = pltpu.get_barrier_semaphore()
@@ -200,18 +233,20 @@
         product = jnp.dot(mixed, pw[group], preferred_element_type=jnp.float32)
         cols = slice(group * GROUP_DIM, (group + 1) * GROUP_DIM)
         pooled[:, cols] = (product * scale_ref[:, cols]).astype(jnp.bfloat16)
-    loads[3].wait()
+    for c in loads[3:]:
+        c.wait()
 
     def project(i, carry):
         at = pl.ds(pl.multiple_of(i * 512, 512), 512)
-        mix[:, at] = jnp.dot(pooled[...], ow[:, at], preferred_element_type=jnp.float32)
+        mix[:, at] = jnp.dot(pooled[...], from_core[:, :, :, at].reshape(pooled.shape[1], 512),
+                             preferred_element_type=jnp.float32)
         return carry
 
     lax.fori_loop(0, width // 512, project, 0)
     loads[2].wait()
 
     def norm_rows(part):
-        begin, count = cuts[part]
+        begin, count = cuts[part][:2]
 
         def body(i, carry):
             at = pl.ds(pl.multiple_of(begin + i * SLOT, SLOT), SLOT)
@@ -225,7 +260,7 @@
 
     def copy(s, t, part, way):
         target = [(grp, sp, tp + 1), (grp, sp, tp - 1), (grp, y_other, tp), (grp, c_other, tp)][way]
-        first, count = cuts[part]
+        first, count = cuts[part][:2]
         piece = every.at[s, t, pl.ds(first, count)]
         return pltpu.make_async_remote_copy(
             src_ref=piece, dst_ref=piece,
@@ -235,143 +270,163 @@
     def arrived(s, t, part):
         copy(s, t, part, 3).wait_recv()
 
-    sent = []
+    def allowed(cond, way):
+        if way == 0:
+            return jnp.logical_and(cond, tp + 1 < n_tp)
+        if way == 1:
+            return jnp.logical_and(cond, tp > 0)
+        return cond
 
     def push(cond, s, t, part, way):
-        if way == 0:
-            cond = jnp.logical_and(cond, tp + 1 < n_tp)
-        if way == 1:
-            cond = jnp.logical_and(cond, tp > 0)
-        pl.when(cond)(lambda: copy(s, t, part, way).start())
-        sent.append((cond, s, t, part, way))
+        pl.when(allowed(cond, way))(lambda: copy(s, t, part, way).start())
 
     def source_rows(s, t):
         return pl.ds(pl.multiple_of((s * n_tp + t) * SLOT, SLOT), SLOT)
 
-    def select(s, t):
-        slot = lax.broadcasted_iota(jnp.int32, (slots, tok), 0).astype(jnp.float32)
+    half = tok // 2
+    rows_h = [pl.ds(h * half, half) for h in range(2)]
+    parts_h = [[p for p, c in enumerate(cuts) if c[2] == h] for h in range(2)]
+    rparts_h = [[p for p, c in enumerate(rcuts) if c[2] == h] for h in range(2)]
+
+    def select(h, s, t):
+        slot = lax.broadcasted_iota(jnp.int32, (slots, half), 0).astype(jnp.float32)
         base = (sp * slots).astype(jnp.float32)
-        meta = metas[s, t]
-        pick = jnp.zeros((slots, tok), jnp.float32)
-        weight = jnp.zeros((slots, tok), jnp.float32)
+        meta = metas[s, t, :, pl.ds(0, half)]
+        pick = jnp.zeros((slots, half), jnp.float32)
+        weight = jnp.zeros((slots, half), jnp.float32)
         for k in range(TOP):
-            hit = (meta[k : k + 1] - base) == slot
+            hit = (meta[4 * h + k : 4 * h + k + 1] - base) == slot
             pick = pick + jnp.where(hit, 1.0, 0.0)
-            weight = weight + jnp.where(hit, meta[TOP + k : TOP + k + 1], 0.0)
+            weight = weight + jnp.where(hit, meta[4 * h + TOP + k : 4 * h + TOP + k + 1], 0.0)
         weight = jnp.broadcast_to(jnp.sum(weight, axis=1, keepdims=True), (slots, 128))
         pick = pick.astype(jnp.bfloat16)
-        picks[s, t] = pick
+        picks[h, s, t] = pick
         for e in range(local_experts):
-            weights[e, source_rows(s, t)] = weight[e * SLOT : (e + 1) * SLOT]
+            weights[h, e, source_rows(s, t)] = weight[e * SLOT : (e + 1) * SLOT]
 
         def body(i, carry):
             at = pl.ds(pl.multiple_of(i * chunk, chunk), chunk)
-            got = jnp.dot(pick, every[s, t, :, at], preferred_element_type=jnp.float32)
+            got = jnp.dot(pick, every[s, t, rows_h[h], at], preferred_element_type=jnp.float32)
             got = got.astype(jnp.bfloat16)
             for e in range(local_experts):
-                held[e, source_rows(s, t), at] = got[e * SLOT : (e + 1) * SLOT]
+                held[h, e, source_rows(s, t), at] = got[e * SLOT : (e + 1) * SLOT]
             return carry
 
         lax.fori_loop(0, width // chunk, body, 0)
 
     yes = tp >= 0
-    norm_rows(0)
-    push(yes, sp, tp, 0, 2)
-    for part in (1, 2):
-        norm_rows(part)
-        push(yes, sp, tp, part, 0)
-        push(yes, sp, tp, part, 1)
-        push(yes, sp, tp, part, 2)
-    push(yes, sp, tp, 0, 0)
-    push(yes, sp, tp, 0, 1)
-    for part in (0, 1, 2):
-        push(yes, sp, tp, part, 3)
-    arrived(y_other, tp, 0)
-    push(yes, y_other, tp, 0, 0)
-    push(yes, y_other, tp, 0, 1)
-    push(yes, y_other, tp, 0, 3)
-    for number, by in enumerate(others):
-        meta_copy(number, by).wait()
-    select(sp, tp)
+    far_core = yo * 2 + (1 - core)
+
+    def own_z(h, parts):
+        for p in parts:
+            push(yes, sp, tp, p, 0)
+            push(yes, sp, tp, p, 1)
+
+    def own_way(h, way):
+        for p in parts_h[h]:
+            push(yes, sp, tp, p, way)
+
+    def crossed(h):
+        p = parts_h[h][0]
+        arrived(y_other, tp, p)
+        push(yes, y_other, tp, p, 0)
+        push(yes, y_other, tp, p, 1)
+        push(yes, y_other, tp, p, 3)
+
+    by_dist = [((tp, yes),)] + [
+        ((tp - d, tp >= d), (tp + d, tp + d < n_tp)) for d in range(1, n_tp)]
 
     def sides(dist):
-        if dist == 0:
-            return ((tp, yes),)
-        return ((tp - dist, tp >= dist), (tp + dist, tp + dist < n_tp))
-
-    def over_y(dist):
+        return by_dist[dist]
+
+    def over_y(h, dist):
         for t, cond in sides(dist):
-            for part in (1, 2):
-                pl.when(cond)(functools.partial(arrived, y_other, t, part))
-                push(cond, y_other, t, part, 3)
-            pl.when(cond)(functools.partial(select, y_other, t))
-
-    def cross(s, t):
-        for part in (0, 1, 2):
-            arrived(s, t, part)
-        select(s, t)
-
-    def over_core(s, dist):
+            for p in parts_h[h][1:]:
+                pl.when(cond)(functools.partial(arrived, y_other, t, p))
+                push(cond, y_other, t, p, 3)
+            pl.when(cond)(functools.partial(select, h, y_other, t))
+
+    def cross(h, s, t):
+        for p in parts_h[h]:
+            arrived(s, t, p)
+        select(h, s, t)
+
+    def over_core(h, s, dist):
         for t, cond in sides(dist):
-            pl.when(cond)(functools.partial(cross, s, t))
-
-    far_core = yo * 2 + (1 - core)
-    for dist in range(1, n_tp):
-        for s, part in ((sp, 1), (sp, 2), (sp, 0), (y_other, 0)):
-            for way, (t, cond) in enumerate(sides(dist)):
-                pl.when(cond)(functools.partial(arrived, s, t, part))
-                push(cond, s, t, part, way)
-                if part:
-                    push(cond, s, t, part, 2)
-                push(cond, s, t, part, 3)
+            pl.when(cond)(functools.partial(cross, h, s, t))
+
+    def along(h, dist, p, s):
+        for way, (t, cond) in enumerate(sides(dist)):
+            pl.when(cond)(functools.partial(arrived, s, t, p))
+            push(cond, s, t, p, way)
+            if p != parts_h[h][0]:
+                push(cond, s, t, p, 2)
+            push(cond, s, t, p, 3)
+
+    def select_along(h, dist):
         for t, cond in sides(dist):
-            pl.when(cond)(functools.partial(select, sp, t))
-        over_core(c_other, dist - 1)
-        over_y(dist - 1)
-        if dist > 1:
-            over_core(far_core, dist - 2)
-    over_core(c_other, n_tp - 1)
-    if n_tp > 1:
-        over_core(far_core, n_tp - 2)
-    over_y(n_tp - 1)
-    over_core(far_core, n_tp - 1)
-    for cond, s, t, part, way in sent:
-        pl.when(cond)(lambda s=s, t=t, part=part, way=way: copy(s, t, part, way).wait_send())
-
-    def expert(e, carry):
+            pl.when(cond)(functools.partial(select, h, sp, t))
+
+    def sent_all(h):
+        head, tail = parts_h[h][0], parts_h[h][1:]
+        sent = [(yes, sp, tp, p, way) for p in parts_h[h] for way in range(4)]
+        sent += [(yes, y_other, tp, head, way) for way in (0, 1, 3)]
+        sent += [(yes, y_other, tp, p, 3) for p in tail]
+        for dist in range(1, n_tp):
+            for side, (t, cond) in enumerate(sides(dist)):
+                sent += [(cond, sp, t, p, way) for p in tail for way in (side, 2, 3)]
+                sent += [(cond, s, t, head, way) for s in (sp, y_other) for way in (side, 3)]
+                sent += [(cond, y_other, t, p, 3) for p in tail]
+        for cond, s, t, p, way in sent:
+            pl.when(allowed(cond, way))(lambda s=s, t=t, p=p, way=way: copy(s, t, p, way).wait_send())
+
+    def use_expert(h, e):
         at = lax.rem(e, buffers)
-        for c in weight_copies(e):
-            c.wait()
-        rows = held[e]
+        rows = held[h, e]
         gate_pre = jnp.dot(rows, wg[at], preferred_element_type=jnp.float32)
         upward = jnp.dot(rows, wu[at], preferred_element_type=jnp.float32)
-        scale = jnp.concatenate([weights[e]] * (gate_pre.shape[1] // 128), axis=1)
+        scale = jnp.concatenate([weights[h, e]] * (gate_pre.shape[1] // 128), axis=1)
         activated = (clamped_unit(gate_pre, upward) * scale).astype(jnp.bfloat16)
 
         def down(i, inner):
             cols = pl.ds(pl.multiple_of(i * chunk, chunk), chunk)
             term = jnp.dot(activated, wd[at, :, cols], preferred_element_type=jnp.float32)
-            held[e, :, cols] = term.astype(jnp.bfloat16)
+            held[h, e, :, cols] = term.astype(jnp.bfloat16)
             return inner
 
         lax.fori_loop(0, width // chunk, down, 0)
 
-        @pl.when(e + buffers < local_experts)
+    def begin_weights(e, cond):
+        @pl.when(cond)
         def _():
-            for c in weight_copies(e + buffers):
+            for c in weight_copies(e):
                 c.start()
 
-        return carry
-
-    lax.fori_loop(0, local_experts, expert, 0)
-
-    def combined(s, t, at):
-        term = held[:, source_rows(s, t), at].reshape(slots, chunk)
-        return lax.dot_general(picks[s, t], term, (((0,), (0,)), ((), ())),
+    def end_weights(e, cond):
+        @pl.when(cond)
+        def _():
+            for c in weight_copies(e):
+                c.wait()
+
+    def experts(h, between):
+        def body(j, carry):
+            e = local_experts - 1 - j if h else j
+            end_weights(e, j >= buffers if h else j >= 0)
+            use_expert(h, e)
+            later = e - buffers if h else e + buffers
+            begin_weights(later, jnp.logical_and(later >= 0, later < local_experts))
+            for number, steps in between:
+                pl.when(j == number)(functools.partial(run, steps))
+            return carry
+
+        lax.fori_loop(0, local_experts, body, 0)
+
+    def combined(h, s, t, at):
+        term = held[h, :, source_rows(s, t), at].reshape(slots, chunk)
+        return lax.dot_general(picks[h, s, t], term, (((0,), (0,)), ((), ())),
                                preferred_element_type=jnp.float32)
 
-    rows_of = [pl.ds(first, count) for first, count in cuts]
-    rows_a = rows_of[0]
+    rows_of = [pl.ds(c[0], c[1]) for c in rcuts]
     ups, downs = (grp, sp, tp + 1), (grp, sp, tp - 1)
     up_ok, down_ok = tp + 1 < n_tp, tp > 0
 
@@ -380,20 +435,20 @@
             src_ref=src, dst_ref=dst, send_sem=s_sem, recv_sem=r_sem,
             device_id=target, device_id_type=MESH)
 
-    def core_copy(y, t):
-        return remote(every.at[y * 2 + (1 - core), t], from_core.at[y, t],
-                      csend.at[y, t], crecv.at[y, t], (grp, c_other, tp))
-
-    def combine_away(y, t):
+    def core_copy(h, y, t):
+        return remote(every.at[y * 2 + (1 - core), t, rows_h[h]], from_core.at[y, t, rows_h[h]],
+                      csend.at[h, y, t], crecv.at[h, y, t], (grp, c_other, tp))
+
+    def combine_away(h, y, t):
         s = y * 2 + (1 - core)
 
         def body(i, carry):
             at = pl.ds(pl.multiple_of(i * chunk, chunk), chunk)
-            every[s, t, :, at] = combined(s, t, at).astype(jnp.bfloat16)
+            every[s, t, rows_h[h], at] = combined(h, s, t, at).astype(jnp.bfloat16)
             return carry
 
         lax.fori_loop(0, width // chunk, body, 0)
-        core_copy(y, t).start()
+        core_copy(h, y, t).start()
 
     order = []
     for dist in range(n_tp - 1, -1, -1):
@@ -401,107 +456,217 @@
             t = tp + side * dist
             order.append((jnp.logical_and(t >= 0, t < n_tp), t, side, dist))
 
-    def y_copy_b(part, t):
-        rows = rows_of[part]
-        return remote(work.at[yo, t, rows], yb.at[t, rows], ysend.at[part, t], yrecv.at[part, t],
+    def y_copy_b(p, t):
+        rows = rows_of[p]
+        return remote(work.at[yo, t, rows], yb.at[t, rows], ysend.at[p, t], yrecv.at[p, t],
                       (grp, y_other, tp))
 
-    def y_copy_a():
-        return remote(work.at[yo, tp, rows_a], ya, ysend.at[0, 0], yrecv.at[0, 0], (grp, y_other, tp))
-
-    def local(y, t):
+    def y_copy_a(h):
+        p = rparts_h[h][0]
+        return remote(work.at[yo, tp, rows_of[p]], ya.at[h, pl.ds(0, rcuts[p][1])], ysend.at[p, 0], yrecv.at[p, 0],
+                      (grp, y_other, tp))
+
+    def local(h, y, t):
         s = y * 2 + core
-        core_copy(y, t).wait_recv()
+        core_copy(h, y, t).wait_recv()
 
         def body(i, carry):
             at = pl.ds(pl.multiple_of(i * chunk, chunk), chunk)
-            both = combined(s, t, at) + from_core[y, t, :, at].astype(jnp.float32)
-            work[y, t, :, at] = both.astype(jnp.bfloat16)
+            both = combined(h, s, t, at) + from_core[y, t, rows_h[h], at].astype(jnp.float32)
+            work[y, t, rows_h[h], at] = both.astype(jnp.bfloat16)
             return carry
 
         lax.fori_loop(0, width // chunk, body, 0)
 
-    def z_ends(part, y, t, slot):
-        rows = rows_of[part]
-        if part:
-            return work.at[y, t, rows], zb.at[slot, rows], bsend.at[part, t], brecv.at[part, slot]
-        return work.at[y, t, rows], za.at[y, slot], asend.at[y, t], arecv.at[y, slot]
-
-    def z_copy(part, y, t, side):
+    def z_ends(p, y, t, slot):
+        rows, h = rows_of[p], rcuts[p][2]
+        if p == rparts_h[h][0]:
+            return work.at[y, t, rows], za.at[h, y, slot, pl.ds(0, rcuts[p][1])], asend.at[h, y, t], arecv.at[h, y, slot]
+        return work.at[y, t, rows], zb.at[slot, rows], bsend.at[p, t], brecv.at[p, slot]
+
+    def z_copy(p, y, t, side):
         if side == 1:
             slot, target = t, ups
         else:
             slot, target = jnp.where(t == tp - 1, n_tp, t), downs
-        return remote(*z_ends(part, y, t, slot), target)
-
-    def take_z(part, y, t, slot):
-        remote(*z_ends(part, y, t, slot), ups).wait_recv()
-        dst, src = z_ends(part, y, t, slot)[:2]
+        return remote(*z_ends(p, y, t, slot), target)
+
+    def take_z(p, y, t, slot):
+        remote(*z_ends(p, y, t, slot), ups).wait_recv()
+        dst, src = z_ends(p, y, t, slot)[:2]
         add_into(dst, src)
 
-    def z_step(part, y, t, side):
+    def z_step(p, y, t, side):
         inner = tp > 0 if side == 1 else tp + 1 < n_tp
-        pl.when(inner)(lambda: take_z(part, y, t, t))
-        z_copy(part, y, t, side).start()
-
-    def z_end(part, y):
-        pl.when(down_ok)(lambda: take_z(part, y, tp, tp))
-        pl.when(up_ok)(lambda: take_z(part, y, tp, n_tp))
-
-    for y in (yo, yy):
+        pl.when(inner)(lambda: take_z(p, y, t, t))
+        z_copy(p, y, t, side).start()
+
+    def z_end(p, y):
+        pl.when(down_ok)(lambda: take_z(p, y, tp, tp))
+        pl.when(up_ok)(lambda: take_z(p, y, tp, n_tp))
+
+    def aways(h, y, want):
         for ok, t, side, dist in order:
-            pl.when(ok)(functools.partial(combine_away, y, t))
-        if y is yo:
-            for ok, t, side, dist in order:
+            if dist == want:
+                pl.when(ok)(functools.partial(combine_away, h, y, t))
+
+    def send_y(h, dists):
+        for ok, t, side, dist in order:
+            if dist in dists:
                 @pl.when(ok)
                 def _(t=t):
-                    local(yo, t)
-                    y_copy_b(1, t).start()
-                    y_copy_b(2, t).start()
-    for ok, t, side, dist in order:
-        @pl.when(ok)
-        def _(t=t, side=side, dist=dist):
-            local(yy, t)
-            if dist:
-                z_step(0, yo, t, side)
-                z_step(0, yy, t, side)
-            for part in (1, 2):
-                y_copy_b(part, t).wait_recv()
-                add_into(work.at[yy, t, rows_of[part]], yb.at[t, rows_of[part]])
+                    local(h, yo, t)
+                    for p in rparts_h[h][1:]:
+                        y_copy_b(p, t).start()
+
+    def reduce_local(h, want):
+        head = rparts_h[h][0]
+        for ok, t, side, dist in order:
+            if dist != want:
+                continue
+
+            @pl.when(ok)
+            def _(t=t, side=side, dist=dist):
+                local(h, yy, t)
                 if dist:
-                    z_step(part, yy, t, side)
-    z_end(0, yo)
-    y_copy_a().start()
-    z_end(0, yy)
-    z_end(1, yy)
-    z_end(2, yy)
-    y_copy_a().wait_recv()
-    add_into(work.at[yy, tp, rows_a], ya)
-    def finish(i, carry):
-        at = pl.ds(pl.multiple_of(i * SLOT, SLOT), SLOT)
-        total = work[yy, tp, at].astype(jnp.float32)
-        out_ref[at] = (residual[at].astype(jnp.float32) + rms_scale(total, pgain_ref[...])).astype(out_ref.dtype)
-        return carry
-
-    lax.fori_loop(0, tok // SLOT, finish, 0)
+                    z_step(head, yo, t, side)
+                    z_step(head, yy, t, side)
+
+    def reduce_part(p, want):
+        for ok, t, side, dist in order:
+            if dist != want:
+                continue
+
+            @pl.when(ok)
+            def _(t=t, side=side, dist=dist):
+                y_copy_b(p, t).wait_recv()
+                add_into(work.at[yy, t, rows_of[p]], yb.at[t, rows_of[p]])
+                if dist:
+                    z_step(p, yy, t, side)
+
+    def reduce_head(h):
+        head = rparts_h[h][0]
+        z_end(head, yo)
+        y_copy_a(h).start()
+        z_end(head, yy)
+
+    def reduce_last(h):
+        head = rparts_h[h][0]
+        y_copy_a(h).wait_recv()
+        add_into(work.at[yy, tp, rows_of[head]], ya.at[h, pl.ds(0, rcuts[head][1])])
+        finish_rows(h)
+
+    def reduce_sent(h):
+        head, tail = rparts_h[h][0], rparts_h[h][1:]
+        y_copy_a(h).wait_send()
+        for ok, t, side, dist in order:
+            @pl.when(ok)
+            def _(t=t, side=side, dist=dist):
+                core_copy(h, yo, t).wait_send()
+                core_copy(h, yy, t).wait_send()
+                for p in tail:
+                    y_copy_b(p, t).wait_send()
+                if dist:
+                    z_copy(head, yo, t, side).wait_send()
+                    z_copy(head, yy, t, side).wait_send()
+                    for p in tail:
+                        z_copy(p, yy, t, side).wait_send()
+
+    def finish_rows(h):
+        def body(i, carry):
+            at = pl.ds(pl.multiple_of(h * half + i * SLOT, SLOT), SLOT)
+            total = work[yy, tp, at].astype(jnp.float32)
+            done = residual[at].astype(jnp.float32) + rms_scale(total, pgain_ref[...])
+            out_ref[at] = done.astype(out_ref.dtype)
+            return carry
+
+        lax.fori_loop(0, half // SLOT, body, 0)
+
+    def step(kind, h, *at):
+        if kind == "N":
+            norm_rows(at[0])
+        elif kind == "OZ":
+            own_z(h, at)
+        elif kind == "OY":
+            push(yes, sp, tp, at[0], 2)
+        elif kind == "OC":
+            own_way(h, 3)
+        elif kind == "X":
+            crossed(h)
+        elif kind == "F":
+            along(h, at[0], at[1], sp if at[2] == "own" else y_other)
+        elif kind == "SA":
+            select_along(h, at[0])
+        elif kind == "YS":
+            over_y(h, at[0])
+        elif kind == "CO":
+            over_core(h, c_other, at[0])
+        elif kind == "FA":
+            over_core(h, far_core, at[0])
+        elif kind == "W":
+            sent_all(h)
+        elif kind == "M":
+            for number, by in enumerate(others):
+                meta_copy(number, by).wait()
+        elif kind == "AW":
+            aways(h, yo if at[0] == "yo" else yy, at[1])
+        elif kind == "SY":
+            send_y(h, at)
+        elif kind == "RL":
+            reduce_local(h, at[0])
+        elif kind == "RT":
+            reduce_part(at[1], at[0])
+        elif kind == "RH":
+            reduce_head(h)
+        elif kind == "RP":
+            z_end(at[0], yy)
+        elif kind == "RF":
+            reduce_last(h)
+
+    def run(steps):
+        for one in steps:
+            step(*one)
+
+    todo, waited = [], set()
+    for one in ORDER:
+        if one[0] == "AW" and one[1] not in waited:
+            waited.add(one[1])
+            todo.append(("W", one[1]))
+        if one[0] in ("SA", "YS", "CO", "FA") and "M" not in waited:
+            waited.add("M")
+            todo.append(("M", 0))
+        todo.append(one)
+    while todo:
+        one = todo.pop(0)
+        if one[0] != "E":
+            step(*one)
+            continue
+        h, between, seen = one[1], [], 0
+        while seen < local_experts - 1:
+            one = todo.pop(0)
+            if one[0] == "E":
+                seen += 1
+            elif between and between[-1][0] == seen:
+                between[-1][1].append(one)
+            else:
+                between.append((seen, [one]))
+        experts(h, between)
+    reduce_sent(0)
+    reduce_sent(1)
     pl.when(has_next)(lambda: halo(tp).wait_send())
     for by in range(1, n_tp):
         to_first = (tp + by) % n_tp == 0
         pl.when(to_first)(lambda by=by: spread(by, False).wait_send())
         pl.when(jnp.logical_not(to_first))(lambda by=by: spread(by, True).wait_send())
-    y_copy_a().wait_send()
-    for ok, t, side, dist in order:
-        @pl.when(ok)
-        def _(t=t, side=side, dist=dist):
-            core_copy(yo, t).wait_send()
-            core_copy(yy, t).wait_send()
-            y_copy_b(1, t).wait_send()
-            y_copy_b(2, t).wait_send()
-            if dist:
-                z_copy(0, yo, t, side).wait_send()
-                z_copy(0, yy, t, side).wait_send()
-                z_copy(1, yy, t, side).wait_send()
-                z_copy(2, yy, t, side).wait_send()
+
+
+def cut_rows(halves):
+    cuts, at = [], 0
+    for h, counts in enumerate(halves):
+        for count in counts:
+            cuts.append((at, count, h))
+            at += count
+    return tuple(cuts)
 
 
 def token_meta(routes_ref, rweight_ref, n_experts):
@@ -512,14 +677,18 @@
                < lax.broadcasted_iota(jnp.int32, (tok, tok), 1))
     earlier = jnp.where(earlier, 1.0, 0.0).astype(jnp.bfloat16)
     before = jnp.dot(sum(hits).astype(jnp.bfloat16), earlier, preferred_element_type=jnp.float32)
-    line = lax.broadcasted_iota(jnp.int32, (8, tok), 0)
-    meta = jnp.zeros((8, tok), jnp.float32)
+    half = tok // 2
+    line = lax.broadcasted_iota(jnp.int32, (8, half), 0)
+    meta = jnp.zeros((8, half), jnp.float32)
     for k in range(TOP):
         rank = jnp.sum(hits[k] * before, axis=0, keepdims=True)
         place = routes_ref[k : k + 1].astype(jnp.float32) * SLOT + rank
-        meta = jnp.where(line == k, place, meta)
-        meta = jnp.where(line == TOP + k, rweight_ref[k : k + 1], meta)
-    return meta
+        weight = rweight_ref[k : k + 1]
+        for h in range(2):
+            lanes = slice(h * half, (h + 1) * half)
+            meta = jnp.where(line == 4 * h + k, place[:, lanes], meta)
+            meta = jnp.where(line == 4 * h + TOP + k, weight[:, lanes], meta)
+    return jnp.concatenate([meta, jnp.zeros((8, tok - half), jnp.float32)], axis=1)
 
 
 def add_into(dst, src):
@@ -539,15 +708,16 @@
     n_tp = lax.axis_size("tp")
     tok, width = resid_in.shape
     local_experts, _, hidden = w_gate.shape
-    cuts = ((0, Y_FIRST), (Y_FIRST, Z_PART), (Y_FIRST + Z_PART, tok - Y_FIRST - Z_PART))
-    an = cuts[0][1]
+    cuts, rcuts = cut_rows(HALVES), cut_rows(BACK)
+    parts, rparts = len(cuts), len(rcuts)
+    heads = [counts[0] for counts in BACK]
     vmem, hbm = pl.BlockSpec(memory_space=pltpu.VMEM), pl.BlockSpec(memory_space=pl.ANY)
     kind = resid_in.dtype
     slots, buffers = local_experts * SLOT, min(4, local_experts)
     channels = pool_input.shape[1]
     dma = pltpu.SemaphoreType.DMA
     return pl.pallas_call(
-        functools.partial(layer_kernel, n_tp, cuts),
+        functools.partial(layer_kernel, n_tp, cuts, rcuts),
         out_shape=jax.ShapeDtypeStruct((tok, width), kind),
         in_specs=[hbm, hbm, vmem, hbm, hbm, vmem, vmem, vmem, vmem, vmem, hbm, hbm, hbm],
         out_specs=vmem,
@@ -555,46 +725,45 @@
             pltpu.VMEM(pool_input.shape, kind),
             pltpu.VMEM((n_tp, tok + SLOT, channels), kind),
             pltpu.VMEM(pool_weight.shape, kind),
-            pltpu.VMEM(out_weight.shape, kind),
             pltpu.VMEM((tok, width), kind),
             pltpu.VMEM((tok, n_tp * channels), kind),
             pltpu.VMEM((tok, width), jnp.float32),
             pltpu.VMEM((4, n_tp, tok, width), kind),
             pltpu.VMEM((4, n_tp, 8, tok), jnp.float32),
-            pltpu.VMEM((4, n_tp, slots, tok), kind),
-            pltpu.VMEM((local_experts, 4 * n_tp * SLOT, 128), jnp.float32),
-            pltpu.VMEM((local_experts, 4 * n_tp * SLOT, width), kind),
+            pltpu.VMEM((2, 4, n_tp, slots, tok // 2), kind),
+            pltpu.VMEM((2, local_experts, 4 * n_tp * SLOT, 128), jnp.float32),
+            pltpu.VMEM((2, local_experts, 4 * n_tp * SLOT, width), kind),
             pltpu.VMEM((buffers, width, hidden), kind),
             pltpu.VMEM((buffers, width, hidden), kind),
             pltpu.VMEM((buffers, hidden, width), kind),
             pltpu.VMEM((2, n_tp, tok, width), kind),
             pltpu.VMEM((2, n_tp, tok, width), kind),
-            pltpu.VMEM((2, n_tp + 1, an, width), kind),
+            pltpu.VMEM((2, 2, n_tp + 1, max(heads), width), kind),
             pltpu.VMEM((n_tp + 1, tok, width), kind),
-            pltpu.VMEM((an, width), kind),
+            pltpu.VMEM((2, max(heads), width), kind),
             pltpu.VMEM((n_tp, tok, width), kind),
             dma((n_tp,)),
             dma((n_tp,)),
             dma((1,)),
             dma((n_tp,)),
-            dma((4,)),
-            dma((4, n_tp, 3, 4)),
-            dma((4, n_tp, 3)),
+            dma((3 + 2 * n_tp,)),
+            dma((4, n_tp, parts, 4)),
+            dma((4, n_tp, parts)),
             dma((4 * n_tp - 1,)),
             dma((4 * n_tp - 1,)),
             dma((3, buffers)),
-            dma((2, n_tp)),
-            dma((2, n_tp)),
-            dma((2, n_tp)),
-            dma((2, n_tp + 1)),
-            dma((3, n_tp)),
-            dma((3, n_tp + 1)),
-            dma((3, n_tp)),
-            dma((3, n_tp)),
+            dma((2, 2, n_tp)),
+            dma((2, 2, n_tp)),
+            dma((2, 2, n_tp)),
+            dma((2, 2, n_tp + 1)),
+            dma((rparts, n_tp)),
+            dma((rparts, n_tp + 1)),
+            dma((rparts, n_tp)),
+            dma((rparts, n_tp)),
             dma((2, max(2, n_tp))),
         ],
         compiler_params=pltpu.CompilerParams(
-            collective_id=0, has_side_effects=True, vmem_limit_bytes=58 * 2**20
+            collective_id=0, has_side_effects=True, vmem_limit_bytes=60 * 2**20
         ),
         name="fused_layer",
     )(pool_input, pool_weight, pool_scale[None], out_weight, resid_in, mix_gain[None], ffn_gain[None],
@@ -629,6 +798,7 @@
         and w_gate.shape[2] <= 256
         and w_gate.shape[0] <= 8
         and width <= 2048
+        and out_weight.shape[0] == 2 * n_tp * tok_rows
     ):
         return fused_layer(resid_in, pool_input, pool_weight, pool_scale, out_weight, mix_gain,
                            ffn_gain, w_gate, w_up, w_down, routes, route_weight, post_gain)

time: 130 us -> 109 us (0.84)
  Pallas kernels: 128 us -> 107 us
    pallas_call x1, Pallas kernels: 128 us -> 107 us  [fused_layer(): pl.pallas_call(functools.partial(layer_kernel, n_tp, cuts, rcuts), out_sh...]
where the time goes in v2:
time: 109 us
  Pallas kernels  107 us (98%)
  local copies, waits for them, and re-layouts  1.88 us (2%)
    pallas_call x1, Pallas kernels, fused_layer(): pl.pallas_call(functools.partial(layer_kernel, n_tp, cuts, rcuts), out_sh...  107 us

profile of v2, /device:TPU:0, one launch (start us, length us, event | category | flops | bytes accessed | tf_op | source)
XLA Modules:
  0.0 109.0 jit_solution(11474603326550714006)
XLA Ops:
  0.0 107.1 %fused_layer.1 = bf16[128,2048]{1,0:T(8,128)(2,1)} custom-call(bf16[512,256]{1,0:T(8,128)(2,1)} %pool_ref.1, bf16[4,256,256]{2,1,0:T(8,128)(2,1)} %pw_ref.1, f32[1,1024]{1,0:T(1,128)} %bitcast.9, bf16[1024,2048]{1,0:T(8,128)(2,1)} %ow_ref.1, bf16[128,2048]{1,0:T(8,128)(2,1)} %resid_ref.1, f32[1,2048]{1,0:T(1,128)} %bitcast.6, f32[1,2048]{1,0:T(1,128)} %bitcast.7, ...), custom_call_target="tpu_custom_call" | custom-call | tf_op jit(solution)/shard_map/fused_layer/pallas_call | solution.py:719
  107.1 1.9 %copy.15 = bf16[128,2048]{1,0:T(8,128)(2,1)} copy(bf16[128,2048]{1,0:T(8,128)(2,1)} %fused_layer.1) | data formatting | bytes 1048576

commit v3 on v2

--- a/solution.py
+++ b/solution.py
@@ -38,37 +38,70 @@
 
 
 SLOT = 16
-HALVES = ((16, 16, 32), (16, 32, 16))
-BACK = ((16, 16, 32), (16, 32, 16))
+HALVES = ((16, 16, 32), (16, 16, 32))
+BACK = ((16, 16, 32), (16, 16, 32))
 ORDER = (
-    ("N", 0, 0), ("OZ", 0, 0), ("N", 0, 2), ("OY", 0, 2), ("N", 1, 4), ("OY", 0, 0), ("N", 1, 5),
-    ("N", 0, 1), ("OZ", 0, 1), ("OY", 0, 1), ("OZ", 0, 2), ("F", 0, 1, 0, "own"), ("N", 1, 3),
-    ("OC", 1), ("F", 0, 1, 1, "own"), ("X", 0), ("F", 0, 2, 0, "own"), ("F", 0, 1, 2, "own"),
-    ("F", 0, 2, 1, "own"), ("F", 0, 2, 2, "own"), ("OC", 0), ("F", 0, 1, 0, "yo"),
-    ("F", 0, 3, 1, "own"), ("YS", 0, 0), ("F", 0, 3, 2, "own"), ("OY", 1, 4), ("SA", 0, 0),
-    ("F", 0, 3, 0, "own"), ("CO", 0, 2), ("SA", 1, 0), ("SA", 0, 2), ("OZ", 1, 5),
-    ("F", 0, 2, 0, "yo"), ("YS", 0, 1), ("YS", 0, 2), ("CO", 0, 3), ("OY", 1, 3), ("OZ", 1, 4),
-    ("CO", 0, 0), ("OZ", 1, 3), ("SA", 0, 3), ("FA", 0, 1), ("OY", 1, 5), ("FA", 0, 2),
-    ("SA", 0, 1), ("F", 0, 3, 0, "yo"), ("YS", 0, 3), ("FA", 0, 0), ("F", 1, 1, 5, "own"),
-    ("FA", 0, 3), ("CO", 0, 1), ("E", 0, 0), ("F", 1, 1, 4, "own"), ("E", 0, 1), ("E", 0, 2),
-    ("X", 1), ("F", 1, 2, 5, "own"), ("E", 0, 3), ("E", 0, 4), ("E", 0, 5), ("F", 1, 2, 4, "own"),
-    ("E", 0, 6), ("E", 0, 7), ("F", 1, 1, 3, "yo"), ("AW", 0, "yo", 3), ("AW", 0, "yo", 2),
-    ("F", 1, 1, 3, "own"), ("AW", 0, "yy", 3), ("F", 1, 3, 5, "own"), ("AW", 0, "yy", 1),
-    ("AW", 0, "yo", 1), ("CO", 1, 0), ("AW", 0, "yy", 2), ("F", 1, 3, 4, "own"), ("SY", 0, 3),
-    ("RL", 0, 3), ("AW", 0, "yy", 0), ("F", 1, 2, 3, "yo"), ("SA", 1, 1), ("YS", 1, 0),
-    ("YS", 1, 2), ("SY", 0, 2), ("F", 1, 2, 3, "own"), ("YS", 1, 1), ("RL", 0, 2), ("SY", 0, 1),
-    ("FA", 1, 2), ("SA", 1, 2), ("FA", 1, 1), ("FA", 1, 0), ("F", 1, 3, 3, "yo"), ("YS", 1, 3),
-    ("F", 1, 3, 3, "own"), ("CO", 1, 1), ("RL", 0, 1), ("FA", 1, 3), ("AW", 0, "yo", 0),
-    ("CO", 1, 3), ("RT", 0, 3, 1), ("CO", 1, 2), ("SA", 1, 3), ("E", 1, 0), ("RT", 0, 3, 2),
-    ("E", 1, 1), ("E", 1, 2), ("RT", 0, 2, 1), ("E", 1, 3), ("E", 1, 4), ("RT", 0, 2, 2),
-    ("SY", 0, 0), ("E", 1, 5), ("E", 1, 6), ("E", 1, 7), ("RT", 0, 1, 1), ("AW", 1, "yo", 3),
-    ("AW", 1, "yy", 0), ("RL", 0, 0), ("AW", 1, "yo", 2), ("RT", 0, 1, 2), ("AW", 1, "yy", 3),
-    ("AW", 1, "yy", 2), ("SY", 1, 3), ("AW", 1, "yo", 1), ("RL", 1, 3), ("RH", 0), ("RT", 0, 0, 2),
-    ("RT", 1, 3, 4), ("SY", 1, 2), ("RT", 1, 3, 5), ("AW", 1, "yy", 1), ("RL", 1, 2),
-    ("RT", 0, 0, 1), ("RP", 0, 1), ("SY", 1, 1), ("RP", 0, 2), ("AW", 1, "yo", 0), ("RF", 0),
-    ("RT", 1, 2, 4), ("RT", 1, 2, 5), ("SY", 1, 0), ("RL", 1, 1), ("RT", 1, 1, 4), ("RL", 1, 0),
-    ("RT", 1, 1, 5), ("RH", 1), ("RT", 1, 0, 5), ("RT", 1, 0, 4), ("RP", 1, 4), ("RP", 1, 5),
-    ("RF", 1),
+    ("P", 0), ("N", 0, 2), ("OY", 0, 2), ("N", 0, 0), ("OY", 0, 0), ("N", 0, 1), ("OZ", 0, 2, 0),
+    ("OZ", 0, 1, 1), ("OZ", 0, 1, 0), ("OY", 0, 1), ("OZ", 0, 0, 1), ("OZ", 0, 2, 1), ("P", 1),
+    ("N", 1, 3), ("SA", 0, 0, 0), ("N", 1, 5), ("OZ", 0, 0, 0), ("F", 0, 1, 1, "own", 1),
+    ("F", 0, 1, 2, "own", 0), ("X", 0), ("F", 0, 1, 1, "own", 0), ("F", 0, 1, 0, "own", 0),
+    ("F", 0, 1, 2, "own", 1), ("YA", 0, 0, 2, 0), ("OC", 0), ("YA", 0, 1, 1, 1), ("CO", 0, 0, 0),
+    ("F", 0, 1, 0, "own", 1), ("SA", 0, 1, 0), ("N", 1, 4), ("F", 0, 2, 2, "own", 0), ("OY", 1, 4),
+    ("SA", 1, 0, 0), ("YA", 0, 0, 1, 0), ("YA", 0, 1, 2, 0), ("OC", 1), ("F", 0, 1, 0, "yo", 0),
+    ("F", 0, 2, 1, "own", 1), ("CO", 0, 1, 0), ("CO", 0, 1, 1), ("CO", 1, 0, 0), ("FA", 0, 0, 0),
+    ("YA", 0, 1, 1, 0), ("YS", 0, 1, 0), ("F", 0, 2, 2, "own", 1), ("YS", 0, 0, 0),
+    ("F", 0, 1, 0, "yo", 1), ("F", 0, 2, 1, "own", 0), ("YA", 0, 1, 2, 1), ("YS", 0, 1, 1),
+    ("SA", 0, 1, 1), ("OZ", 1, 4, 1), ("OY", 1, 3), ("FA", 0, 1, 0), ("F", 0, 2, 0, "own", 0),
+    ("FA", 0, 1, 1), ("F", 0, 3, 1, "own", 1), ("E", 0, 0), ("F", 0, 2, 0, "own", 1),
+    ("SA", 0, 2, 1), ("E", 0, 0), ("E", 0, 0), ("F", 0, 3, 2, "own", 0), ("F", 0, 2, 0, "yo", 0),
+    ("E", 0, 0), ("F", 0, 3, 2, "own", 1), ("OZ", 1, 4, 0), ("YA", 0, 2, 2, 0), ("E", 0, 0),
+    ("F", 0, 2, 0, "yo", 1), ("F", 0, 3, 1, "own", 0), ("YA", 1, 0, 4, 0), ("OY", 1, 5),
+    ("YA", 0, 3, 1, 1), ("YA", 0, 2, 2, 1), ("YA", 0, 2, 1, 1), ("OZ", 1, 5, 0), ("OZ", 1, 5, 1),
+    ("E", 0, 0), ("YA", 0, 2, 1, 0), ("F", 1, 1, 4, "own", 1), ("E", 0, 0), ("YA", 0, 3, 2, 0),
+    ("F", 0, 3, 0, "own", 0), ("E", 0, 0), ("CO", 0, 2, 0), ("F", 0, 3, 0, "own", 1),
+    ("CO", 0, 2, 1), ("FA", 0, 2, 1), ("YA", 0, 3, 2, 1), ("FA", 0, 2, 0), ("YA", 0, 3, 1, 0),
+    ("F", 0, 3, 0, "yo", 0), ("SA", 0, 3, 1), ("F", 0, 3, 0, "yo", 1), ("SA", 0, 3, 0),
+    ("YS", 0, 3, 1), ("CO", 0, 3, 1), ("CO", 0, 3, 0), ("SA", 0, 2, 0), ("YS", 0, 2, 0),
+    ("F", 1, 1, 4, "own", 0), ("YS", 0, 2, 1), ("FA", 0, 3, 1), ("FA", 0, 3, 0), ("YS", 0, 3, 0),
+    ("E", 0, 1), ("E", 0, 1), ("F", 1, 1, 5, "own", 1), ("OZ", 1, 3, 1), ("YA", 1, 0, 5, 0),
+    ("F", 1, 1, 5, "own", 0), ("E", 0, 1), ("E", 0, 1), ("OZ", 1, 3, 0), ("X", 1),
+    ("F", 1, 2, 4, "own", 0), ("F", 1, 2, 4, "own", 1), ("YA", 1, 1, 4, 1), ("E", 0, 1),
+    ("E", 0, 1), ("E", 0, 1), ("F", 1, 2, 5, "own", 1), ("E", 0, 1), ("AW", 0, "yo", 3, 0),
+    ("F", 1, 2, 5, "own", 0), ("AW", 0, "yy", 3, 0), ("YA", 1, 1, 4, 0), ("AW", 0, "yy", 2, 0),
+    ("F", 1, 1, 3, "own", 1), ("AW", 0, "yy", 1, 0), ("AW", 0, "yo", 3, 1), ("FA", 1, 0, 0),
+    ("AW", 0, "yy", 3, 1), ("AW", 0, "yo", 0, 0), ("AW", 0, "yo", 1, 1), ("F", 1, 1, 3, "own", 0),
+    ("SY", 0, 3, 0), ("F", 1, 1, 3, "yo", 1), ("SA", 1, 1, 1), ("YA", 1, 1, 5, 1), ("RL", 0, 3, 0),
+    ("AW", 0, "yy", 1, 1), ("YS", 1, 0, 0), ("SA", 1, 1, 0), ("F", 1, 1, 3, "yo", 0),
+    ("AW", 0, "yo", 2, 0), ("SY", 0, 3, 1), ("RL", 0, 3, 1), ("YA", 1, 1, 5, 0), ("YS", 1, 1, 1),
+    ("AW", 0, "yo", 1, 0), ("YS", 1, 1, 0), ("AW", 0, "yo", 2, 1), ("CO", 1, 1, 1),
+    ("AW", 0, "yy", 2, 1), ("CO", 1, 1, 0), ("FA", 1, 1, 1), ("FA", 1, 1, 0), ("E", 1, 0),
+    ("E", 1, 0), ("RT", 0, 3, 1, 0), ("F", 1, 3, 4, "own", 0), ("F", 1, 3, 4, "own", 1),
+    ("YA", 1, 2, 4, 0), ("RT", 0, 3, 1, 1), ("F", 1, 3, 5, "own", 1), ("SY", 0, 2, 0), ("E", 1, 0),
+    ("F", 1, 3, 5, "own", 0), ("RL", 0, 2, 0), ("SY", 0, 2, 1), ("RL", 0, 2, 1), ("YA", 1, 2, 4, 1),
+    ("F", 1, 2, 3, "own", 1), ("F", 1, 2, 3, "own", 0), ("E", 1, 0), ("YA", 1, 2, 5, 0),
+    ("E", 1, 0), ("RT", 0, 3, 2, 0), ("F", 1, 2, 3, "yo", 0), ("RT", 0, 3, 2, 1),
+    ("F", 1, 2, 3, "yo", 1), ("SY", 0, 1, 0), ("SY", 0, 1, 1), ("E", 1, 0), ("E", 1, 0),
+    ("RL", 0, 1, 0), ("YA", 1, 2, 5, 1), ("RL", 0, 1, 1), ("CO", 1, 2, 0), ("YA", 1, 3, 4, 0),
+    ("CO", 1, 2, 1), ("E", 1, 0), ("F", 1, 3, 3, "own", 1), ("F", 1, 3, 3, "own", 0),
+    ("YA", 1, 3, 4, 1), ("YA", 1, 3, 5, 1), ("SY", 0, 0, 0), ("F", 1, 3, 3, "yo", 1),
+    ("FA", 1, 2, 1), ("SA", 1, 3, 1), ("SA", 1, 3, 0), ("F", 1, 3, 3, "yo", 0), ("YA", 1, 3, 5, 0),
+    ("CO", 1, 3, 1), ("CO", 1, 3, 0), ("YS", 1, 3, 0), ("SA", 1, 2, 0), ("RT", 0, 2, 1, 0),
+    ("FA", 1, 2, 0), ("RT", 0, 2, 1, 1), ("YS", 1, 3, 1), ("YS", 1, 2, 1), ("SA", 1, 2, 1),
+    ("FA", 1, 3, 1), ("YS", 1, 2, 0), ("FA", 1, 3, 0), ("E", 1, 1), ("E", 1, 1), ("RT", 0, 2, 2, 1),
+    ("RT", 0, 2, 2, 0), ("E", 1, 1), ("E", 1, 1), ("E", 1, 1), ("E", 1, 1), ("RT", 0, 1, 1, 0),
+    ("RT", 0, 1, 1, 1), ("E", 1, 1), ("E", 1, 1), ("RT", 0, 1, 2, 1), ("AW", 1, "yo", 3, 0),
+    ("AW", 1, "yo", 3, 1), ("RT", 0, 1, 2, 0), ("AW", 1, "yy", 3, 1), ("AW", 1, "yy", 3, 0),
+    ("AW", 1, "yy", 2, 1), ("AW", 1, "yo", 2, 0), ("AW", 0, "yy", 0, 0), ("SY", 1, 3, 0),
+    ("SY", 1, 3, 1), ("RL", 1, 3, 1), ("RL", 1, 3, 0), ("AW", 1, "yy", 2, 0), ("AW", 1, "yo", 1, 0),
+    ("AW", 1, "yo", 1, 1), ("AW", 1, "yo", 2, 1), ("SY", 1, 2, 0), ("RT", 1, 3, 4, 1),
+    ("RT", 1, 3, 4, 0), ("RL", 0, 0, 0), ("RH", 0), ("SY", 1, 2, 1), ("RL", 1, 2, 1),
+    ("AW", 1, "yy", 1, 1), ("RT", 0, 0, 1, 0), ("SY", 1, 1, 0), ("AW", 1, "yo", 0, 0),
+    ("SY", 1, 1, 1), ("RT", 1, 3, 5, 0), ("AW", 1, "yy", 1, 0), ("RT", 1, 3, 5, 1), ("RL", 1, 2, 0),
+    ("RL", 1, 1, 1), ("AW", 1, "yy", 0, 0), ("RT", 1, 2, 4, 1), ("RP", 0, 1), ("RT", 0, 0, 2, 0),
+    ("RT", 1, 2, 5, 0), ("SY", 1, 0, 0), ("RT", 1, 2, 4, 0), ("RL", 1, 1, 0), ("RP", 0, 2),
+    ("RF", 0), ("RT", 1, 2, 5, 1), ("RT", 1, 1, 5, 0), ("RT", 1, 1, 4, 1), ("RT", 1, 1, 4, 0),
+    ("RT", 1, 1, 5, 1), ("RL", 1, 0, 0), ("RT", 1, 0, 4, 0), ("RH", 1), ("RT", 1, 0, 5, 0),
+    ("RP", 1, 5), ("RP", 1, 4), ("RF", 1),
 )
 MESH = pl.DeviceIdType.MESH
 
@@ -161,23 +194,29 @@
     rest = tp > 0
     has_next = sp + 1 < 4
 
-    def ends(to, whole, chan):
+    half = tok // 2
+    rows_h = [pl.ds(h * half, half) for h in range(2)]
+
+    def ends(h, to, whole, chan):
+        if h:
+            at = pl.multiple_of(to * tok + half, half)
+            return pool.at[pl.ds(at, half)], rows_in.at[chan, pl.ds(reach + half, half)]
         if whole:
             at = pl.multiple_of(to * tok - reach, reach)
-            return pool.at[pl.ds(at, tok + reach)], rows_in.at[chan]
-        return pool.at[pl.ds(0, tok)], rows_in.at[chan, pl.ds(reach, tok)]
-
-    def spread(by, whole):
+            return pool.at[pl.ds(at, half + reach)], rows_in.at[chan, pl.ds(0, half + reach)]
+        return pool.at[pl.ds(0, half)], rows_in.at[chan, pl.ds(reach, half)]
+
+    def spread(h, by, whole):
         to = (tp + by) % n_tp
-        src, dst = ends(to, whole, tp)
+        src, dst = ends(h, to, whole, tp)
         return pltpu.make_async_remote_copy(
-            src_ref=src, dst_ref=dst, send_sem=psend.at[by], recv_sem=precv.at[tp],
+            src_ref=src, dst_ref=dst, send_sem=psend.at[h, by], recv_sem=precv.at[h, tp],
             device_id=(grp, sp, to), device_id_type=MESH)
 
-    def landed(chan, whole):
-        src, dst = ends(1 if whole else 0, whole, chan)
+    def landed(h, chan, whole):
+        src, dst = ends(h, 1 if whole else 0, whole, chan)
         return pltpu.make_async_remote_copy(
-            src_ref=src, dst_ref=dst, send_sem=psend.at[0], recv_sem=precv.at[chan],
+            src_ref=src, dst_ref=dst, send_sem=psend.at[h, 0], recv_sem=precv.at[h, chan],
             device_id=(grp, sp, tp), device_id_type=MESH)
 
     def halo(chan):
@@ -187,17 +226,27 @@
             send_sem=hsend.at[0], recv_sem=hrecv.at[chan],
             device_id=(grp, sp + 1, 0), device_id_type=MESH)
 
-    def kept(whole):
-        src, dst = ends(tp, whole, tp)
-        return pltpu.make_async_copy(src, dst, own.at[0, 1])
+    def kept(h, whole):
+        src, dst = ends(h, tp, whole, tp)
+        return pltpu.make_async_copy(src, dst, own.at[h, 1])
+
+    def each_spread(act):
+        for h in range(2):
+            for by in range(n_tp - 1, 0, -1):
+                for to in (tp + by, tp - by):
+                    rank = lax.rem(to - tp + n_tp, n_tp)
+                    good = jnp.logical_and(to >= 0, to < n_tp)
+                    if h:
+                        pl.when(good)(lambda r=rank: act(spread(1, r, True)))
+                        continue
+                    pl.when(jnp.logical_and(good, to == 0))(lambda r=rank: act(spread(0, r, False)))
+                    pl.when(jnp.logical_and(good, to > 0))(lambda r=rank: act(spread(0, r, True)))
 
     pl.when(has_next)(lambda: halo(tp).start())
-    for by in range(1, n_tp):
-        to_first = (tp + by) % n_tp == 0
-        pl.when(to_first)(lambda by=by: spread(by, False).start())
-        pl.when(jnp.logical_not(to_first))(lambda by=by: spread(by, True).start())
-    pl.when(first)(lambda: kept(False).start())
-    pl.when(rest)(lambda: kept(True).start())
+    each_spread(lambda c: c.start())
+    pl.when(first)(lambda: kept(0, False).start())
+    pl.when(rest)(lambda: kept(0, True).start())
+    kept(1, True).start()
     for number, by in enumerate(others):
         meta_copy(number, by).start()
     for e in range(min(buffers, local_experts)):
@@ -209,41 +258,51 @@
         for chan in range(n_tp):
             rows_in[chan, pl.ds(0, reach)] = jnp.zeros((reach, rows_in.shape[2]), rows_in.dtype)
 
-    loads[1].wait()
     start = (sp * n_tp + tp) * tok
-    for group, window in enumerate(pool_windows):
+
+    def pool_group(h, group, window):
         mine = tp == group
-        if group:
-            pl.when(mine)(lambda: kept(True).wait())
-            pl.when(first)(lambda g=group: landed(g, False).wait_recv())
-            pl.when(jnp.logical_and(rest, tp != group))(lambda g=group: landed(g, True).wait_recv())
+        if h:
+            pl.when(mine)(lambda: kept(1, True).wait())
+            pl.when(tp != group)(lambda: landed(1, group, True).wait_recv())
         else:
-            pl.when(mine)(lambda: kept(False).wait())
-            pl.when(rest)(lambda: landed(0, True).wait_recv())
-        pl.when(jnp.logical_and(first, sp > 0))(lambda g=group: halo(g).wait_recv())
-        values = rows_in[group].astype(jnp.float32)
+            pl.when(mine)(lambda: kept(0, group > 0).wait())
+            if group:
+                pl.when(first)(lambda: landed(0, group, False).wait_recv())
+                pl.when(jnp.logical_and(rest, tp != group))(lambda: landed(0, group, True).wait_recv())
+            else:
+                pl.when(rest)(lambda: landed(0, 0, True).wait_recv())
+            pl.when(jnp.logical_and(first, sp > 0))(lambda: halo(group).wait_recv())
+        values = rows_in[group, pl.ds(h * half, half + reach)].astype(jnp.float32)
         total = values
         span = 1
         while span < window:
             total = total + jnp.concatenate([total[:span], total[:-span]], axis=0)
             span *= 2
-        count = start + lax.broadcasted_iota(jnp.int32, (tok, values.shape[1]), 0) + 1
+        count = start + h * half + lax.broadcasted_iota(jnp.int32, (half, values.shape[1]), 0) + 1
         divisor = jnp.minimum(count, window).astype(jnp.float32)
         mixed = (total[reach:] / divisor - values[reach:]).astype(jnp.bfloat16)
         product = jnp.dot(mixed, pw[group], preferred_element_type=jnp.float32)
         cols = slice(group * GROUP_DIM, (group + 1) * GROUP_DIM)
-        pooled[:, cols] = (product * scale_ref[:, cols]).astype(jnp.bfloat16)
-    for c in loads[3:]:
-        c.wait()
-
-    def project(i, carry):
-        at = pl.ds(pl.multiple_of(i * 512, 512), 512)
-        mix[:, at] = jnp.dot(pooled[...], from_core[:, :, :, at].reshape(pooled.shape[1], 512),
-                             preferred_element_type=jnp.float32)
-        return carry
-
-    lax.fori_loop(0, width // 512, project, 0)
-    loads[2].wait()
+        pooled[rows_h[h], cols] = (product * scale_ref[:, cols]).astype(jnp.bfloat16)
+
+    def pool_half(h):
+        if h == 0:
+            loads[1].wait()
+        for group, window in enumerate(pool_windows):
+            pool_group(h, group, window)
+        if h == 0:
+            for c in loads[2:]:
+                c.wait()
+
+        def project(i, carry):
+            at = pl.ds(pl.multiple_of(i * 1024, 1024), 1024)
+            mix[rows_h[h], at] = jnp.dot(
+                pooled[rows_h[h]], from_core[:, :, :, at].reshape(pooled.shape[1], 1024),
+                preferred_element_type=jnp.float32)
+            return carry
+
+        lax.fori_loop(0, width // 1024, project, 0)
 
     def norm_rows(part):
         begin, count = cuts[part][:2]
@@ -281,7 +340,7 @@
         pl.when(allowed(cond, way))(lambda: copy(s, t, part, way).start())
 
     def source_rows(s, t):
-        return pl.ds(pl.multiple_of((s * n_tp + t) * SLOT, SLOT), SLOT)
+        return pl.ds(pl.multiple_of((t * 4 + s) * SLOT, SLOT), SLOT)
 
     half = tok // 2
     rows_h = [pl.ds(h * half, half) for h in range(2)]
@@ -291,13 +350,13 @@
     def select(h, s, t):
         slot = lax.broadcasted_iota(jnp.int32, (slots, half), 0).astype(jnp.float32)
         base = (sp * slots).astype(jnp.float32)
-        meta = metas[s, t, :, pl.ds(0, half)]
+        meta = metas[s, t][:, h * half : (h + 1) * half]
         pick = jnp.zeros((slots, half), jnp.float32)
         weight = jnp.zeros((slots, half), jnp.float32)
         for k in range(TOP):
-            hit = (meta[4 * h + k : 4 * h + k + 1] - base) == slot
+            hit = (meta[k : k + 1] - base) == slot
             pick = pick + jnp.where(hit, 1.0, 0.0)
-            weight = weight + jnp.where(hit, meta[4 * h + TOP + k : 4 * h + TOP + k + 1], 0.0)
+            weight = weight + jnp.where(hit, meta[TOP + k : TOP + k + 1], 0.0)
         weight = jnp.broadcast_to(jnp.sum(weight, axis=1, keepdims=True), (slots, 128))
         pick = pick.astype(jnp.bfloat16)
         picks[h, s, t] = pick
@@ -317,11 +376,6 @@
     yes = tp >= 0
     far_core = yo * 2 + (1 - core)
 
-    def own_z(h, parts):
-        for p in parts:
-            push(yes, sp, tp, p, 0)
-            push(yes, sp, tp, p, 1)
-
     def own_way(h, way):
         for p in parts_h[h]:
             push(yes, sp, tp, p, way)
@@ -339,33 +393,31 @@
     def sides(dist):
         return by_dist[dist]
 
-    def over_y(h, dist):
-        for t, cond in sides(dist):
-            for p in parts_h[h][1:]:
-                pl.when(cond)(functools.partial(arrived, y_other, t, p))
-                push(cond, y_other, t, p, 3)
-            pl.when(cond)(functools.partial(select, h, y_other, t))
+    def over_y(h, dist, p, side):
+        t, cond = sides(dist)[side]
+        pl.when(cond)(functools.partial(arrived, y_other, t, p))
+        push(cond, y_other, t, p, 3)
+
+    def select_from(h, s, dist, side):
+        t, cond = sides(dist)[side]
+        pl.when(cond)(functools.partial(select, h, s, t))
 
     def cross(h, s, t):
         for p in parts_h[h]:
             arrived(s, t, p)
         select(h, s, t)
 
-    def over_core(h, s, dist):
-        for t, cond in sides(dist):
-            pl.when(cond)(functools.partial(cross, h, s, t))
-
-    def along(h, dist, p, s):
-        for way, (t, cond) in enumerate(sides(dist)):
-            pl.when(cond)(functools.partial(arrived, s, t, p))
-            push(cond, s, t, p, way)
-            if p != parts_h[h][0]:
-                push(cond, s, t, p, 2)
-            push(cond, s, t, p, 3)
-
-    def select_along(h, dist):
-        for t, cond in sides(dist):
-            pl.when(cond)(functools.partial(select, h, sp, t))
+    def over_core(h, s, dist, side):
+        t, cond = sides(dist)[side]
+        pl.when(cond)(functools.partial(cross, h, s, t))
+
+    def along(h, dist, p, s, side):
+        t, cond = sides(dist)[side]
+        pl.when(cond)(functools.partial(arrived, s, t, p))
+        push(cond, s, t, p, side)
+        if p != parts_h[h][0]:
+            push(cond, s, t, p, 2)
+        push(cond, s, t, p, 3)
 
     def sent_all(h):
         head, tail = parts_h[h][0], parts_h[h][1:]
@@ -380,21 +432,15 @@
         for cond, s, t, p, way in sent:
             pl.when(allowed(cond, way))(lambda s=s, t=t, p=p, way=way: copy(s, t, p, way).wait_send())
 
-    def use_expert(h, e):
+    def use_expert(h, e, at_rows):
         at = lax.rem(e, buffers)
-        rows = held[h, e]
+        rows = held[h, e, at_rows]
         gate_pre = jnp.dot(rows, wg[at], preferred_element_type=jnp.float32)
         upward = jnp.dot(rows, wu[at], preferred_element_type=jnp.float32)
-        scale = jnp.concatenate([weights[h, e]] * (gate_pre.shape[1] // 128), axis=1)
+        scale = jnp.concatenate([weights[h, e, at_rows]] * (gate_pre.shape[1] // 128), axis=1)
         activated = (clamped_unit(gate_pre, upward) * scale).astype(jnp.bfloat16)
-
-        def down(i, inner):
-            cols = pl.ds(pl.multiple_of(i * chunk, chunk), chunk)
-            term = jnp.dot(activated, wd[at, :, cols], preferred_element_type=jnp.float32)
-            held[h, e, :, cols] = term.astype(jnp.bfloat16)
-            return inner
-
-        lax.fori_loop(0, width // chunk, down, 0)
+        term = jnp.dot(activated, wd[at], preferred_element_type=jnp.float32)
+        held[h, e, at_rows] = term.astype(jnp.bfloat16)
 
     def begin_weights(e, cond):
         @pl.when(cond)
@@ -408,12 +454,19 @@
             for c in weight_copies(e):
                 c.wait()
 
-    def experts(h, between):
+    def experts(h, far, between):
+        pair = n_tp // 2
+        group = tp // pair
+        group = 1 - group if far else group
+        count = pair * 4 * SLOT
+        at_rows = pl.ds(pl.multiple_of(group * count, count), count)
+        fresh = h == 0 and not far
+
         def body(j, carry):
-            e = local_experts - 1 - j if h else j
-            end_weights(e, j >= buffers if h else j >= 0)
-            use_expert(h, e)
-            later = e - buffers if h else e + buffers
+            e = local_experts - 1 - j if far else j
+            end_weights(e, j >= (0 if fresh else buffers))
+            use_expert(h, e, at_rows)
+            later = e - buffers if far else e + buffers
             begin_weights(later, jnp.logical_and(later >= 0, later < local_experts))
             for number, steps in between:
                 pl.when(j == number)(functools.partial(run, steps))
@@ -454,7 +507,7 @@
     for dist in range(n_tp - 1, -1, -1):
         for side in (1, -1) if dist else (1,):
             t = tp + side * dist
-            order.append((jnp.logical_and(t >= 0, t < n_tp), t, side, dist))
+            order.append((jnp.logical_and(t >= 0, t < n_tp), t, side, (dist, int(side < 0))))
 
     def y_copy_b(p, t):
         rows = rows_of[p]
@@ -512,7 +565,7 @@
 
     def send_y(h, dists):
         for ok, t, side, dist in order:
-            if dist in dists:
+            if dist == dists:
                 @pl.when(ok)
                 def _(t=t):
                     local(h, yo, t)
@@ -528,7 +581,7 @@
             @pl.when(ok)
             def _(t=t, side=side, dist=dist):
                 local(h, yy, t)
-                if dist:
+                if dist[0]:
                     z_step(head, yo, t, side)
                     z_step(head, yy, t, side)
 
@@ -541,7 +594,7 @@
             def _(t=t, side=side, dist=dist):
                 y_copy_b(p, t).wait_recv()
                 add_into(work.at[yy, t, rows_of[p]], yb.at[t, rows_of[p]])
-                if dist:
+                if dist[0]:
                     z_step(p, yy, t, side)
 
     def reduce_head(h):
@@ -566,7 +619,7 @@
                 core_copy(h, yy, t).wait_send()
                 for p in tail:
                     y_copy_b(p, t).wait_send()
-                if dist:
+                if dist[0]:
                     z_copy(head, yo, t, side).wait_send()
                     z_copy(head, yy, t, side).wait_send()
                     for p in tail:
@@ -583,10 +636,12 @@
         lax.fori_loop(0, half // SLOT, body, 0)
 
     def step(kind, h, *at):
-        if kind == "N":
+        if kind == "P":
+            pool_half(h)
+        elif kind == "N":
             norm_rows(at[0])
         elif kind == "OZ":
-            own_z(h, at)
+            push(yes, sp, tp, at[0], at[1])
         elif kind == "OY":
             push(yes, sp, tp, at[0], 2)
         elif kind == "OC":
@@ -594,28 +649,30 @@
         elif kind == "X":
             crossed(h)
         elif kind == "F":
-            along(h, at[0], at[1], sp if at[2] == "own" else y_other)
+            along(h, at[0], at[1], sp if at[2] == "own" else y_other, at[3])
         elif kind == "SA":
-            select_along(h, at[0])
+            select_from(h, sp, *at)
+        elif kind == "YA":
+            over_y(h, *at)
         elif kind == "YS":
-            over_y(h, at[0])
+            select_from(h, y_other, *at)
         elif kind == "CO":
-            over_core(h, c_other, at[0])
+            over_core(h, c_other, *at)
         elif kind == "FA":
-            over_core(h, far_core, at[0])
+            over_core(h, far_core, *at)
         elif kind == "W":
             sent_all(h)
         elif kind == "M":
             for number, by in enumerate(others):
                 meta_copy(number, by).wait()
         elif kind == "AW":
-            aways(h, yo if at[0] == "yo" else yy, at[1])
+            aways(h, yo if at[0] == "yo" else yy, at[1:])
         elif kind == "SY":
             send_y(h, at)
         elif kind == "RL":
-            reduce_local(h, at[0])
+            reduce_local(h, at)
         elif kind == "RT":
-            reduce_part(at[1], at[0])
+            reduce_part(at[1], (at[0], at[2]))
         elif kind == "RH":
             reduce_head(h)
         elif kind == "RP":
@@ -641,7 +698,7 @@
         if one[0] != "E":
             step(*one)
             continue
-        h, between, seen = one[1], [], 0
+        h, far, between, seen = one[1], one[2] > 0, [], 0
         while seen < local_experts - 1:
             one = todo.pop(0)
             if one[0] == "E":
@@ -650,14 +707,11 @@
                 between[-1][1].append(one)
             else:
                 between.append((seen, [one]))
-        experts(h, between)
+        experts(h, far, between)
     reduce_sent(0)
     reduce_sent(1)
     pl.when(has_next)(lambda: halo(tp).wait_send())
-    for by in range(1, n_tp):
-        to_first = (tp + by) % n_tp == 0
-        pl.when(to_first)(lambda by=by: spread(by, False).wait_send())
-        pl.when(jnp.logical_not(to_first))(lambda by=by: spread(by, True).wait_send())
+    each_spread(lambda c: c.wait_send())
 
 
 def cut_rows(halves):
@@ -677,18 +731,14 @@
                < lax.broadcasted_iota(jnp.int32, (tok, tok), 1))
     earlier = jnp.where(earlier, 1.0, 0.0).astype(jnp.bfloat16)
     before = jnp.dot(sum(hits).astype(jnp.bfloat16), earlier, preferred_element_type=jnp.float32)
-    half = tok // 2
-    line = lax.broadcasted_iota(jnp.int32, (8, half), 0)
-    meta = jnp.zeros((8, half), jnp.float32)
+    line = lax.broadcasted_iota(jnp.int32, (2 * TOP, tok), 0)
+    meta = jnp.zeros((2 * TOP, tok), jnp.float32)
     for k in range(TOP):
         rank = jnp.sum(hits[k] * before, axis=0, keepdims=True)
         place = routes_ref[k : k + 1].astype(jnp.float32) * SLOT + rank
-        weight = rweight_ref[k : k + 1]
-        for h in range(2):
-            lanes = slice(h * half, (h + 1) * half)
-            meta = jnp.where(line == 4 * h + k, place[:, lanes], meta)
-            meta = jnp.where(line == 4 * h + TOP + k, weight[:, lanes], meta)
-    return jnp.concatenate([meta, jnp.zeros((8, tok - half), jnp.float32)], axis=1)
+        meta = jnp.where(line == k, place, meta)
+        meta = jnp.where(line == TOP + k, rweight_ref[k : k + 1], meta)
+    return meta
 
 
 def add_into(dst, src):
@@ -729,7 +779,7 @@
             pltpu.VMEM((tok, n_tp * channels), kind),
             pltpu.VMEM((tok, width), jnp.float32),
             pltpu.VMEM((4, n_tp, tok, width), kind),
-            pltpu.VMEM((4, n_tp, 8, tok), jnp.float32),
+            pltpu.VMEM((4, n_tp, 2 * TOP, tok), jnp.float32),
             pltpu.VMEM((2, 4, n_tp, slots, tok // 2), kind),
             pltpu.VMEM((2, local_experts, 4 * n_tp * SLOT, 128), jnp.float32),
             pltpu.VMEM((2, local_experts, 4 * n_tp * SLOT, width), kind),
@@ -742,8 +792,8 @@
             pltpu.VMEM((n_tp + 1, tok, width), kind),
             pltpu.VMEM((2, max(heads), width), kind),
             pltpu.VMEM((n_tp, tok, width), kind),
-            dma((n_tp,)),
-            dma((n_tp,)),
+            dma((2, n_tp)),
+            dma((2, n_tp)),
             dma((1,)),
             dma((n_tp,)),
             dma((3 + 2 * n_tp,)),

time: 109 us -> 106 us (0.972)
  Pallas kernels: 107 us -> 104 us
    pallas_call x1, Pallas kernels: 107 us -> 104 us  [fused_layer(): pl.pallas_call(functools.partial(layer_kernel, n_tp, cuts, rcuts), out_sh...]
where the time goes in v3:
time: 106 us
  Pallas kernels  104 us (98%)
  local copies, waits for them, and re-layouts  1.88 us (2%)
    pallas_call x1, Pallas kernels, fused_layer(): pl.pallas_call(functools.partial(layer_kernel, n_tp, cuts, rcuts), out_sh...  104 us

profile of v3, /device:TPU:0, one launch (start us, length us, event | category | flops | bytes accessed | tf_op | source)
XLA Modules:
  0.0 105.9 jit_solution(7162568894255958236)
XLA Ops:
  0.0 104.0 %fused_layer.1 = bf16[128,2048]{1,0:T(8,128)(2,1)} custom-call(bf16[512,256]{1,0:T(8,128)(2,1)} %pool_ref.1, bf16[4,256,256]{2,1,0:T(8,128)(2,1)} %pw_ref.1, f32[1,1024]{1,0:T(1,128)} %bitcast.9, bf16[1024,2048]{1,0:T(8,128)(2,1)} %ow_ref.1, bf16[128,2048]{1,0:T(8,128)(2,1)} %resid_ref.1, f32[1,2048]{1,0:T(1,128)} %bitcast.6, f32[1,2048]{1,0:T(1,128)} %bitcast.7, ...), custom_call_target="tpu_custom_call" | custom-call | tf_op jit(solution)/shard_map/fused_layer/pallas_call | solution.py:769
  104.0 1.9 %copy.15 = bf16[128,2048]{1,0:T(8,128)(2,1)} copy(bf16[128,2048]{1,0:T(8,128)(2,1)} %fused_layer.1) | data formatting | bytes 1048576

commit v4 on v3

--- a/solution.py
+++ b/solution.py
@@ -41,67 +41,68 @@
 HALVES = ((16, 16, 32), (16, 16, 32))
 BACK = ((16, 16, 32), (16, 16, 32))
 ORDER = (
-    ("P", 0), ("N", 0, 2), ("OY", 0, 2), ("N", 0, 0), ("OY", 0, 0), ("N", 0, 1), ("OZ", 0, 2, 0),
-    ("OZ", 0, 1, 1), ("OZ", 0, 1, 0), ("OY", 0, 1), ("OZ", 0, 0, 1), ("OZ", 0, 2, 1), ("P", 1),
-    ("N", 1, 3), ("SA", 0, 0, 0), ("N", 1, 5), ("OZ", 0, 0, 0), ("F", 0, 1, 1, "own", 1),
-    ("F", 0, 1, 2, "own", 0), ("X", 0), ("F", 0, 1, 1, "own", 0), ("F", 0, 1, 0, "own", 0),
-    ("F", 0, 1, 2, "own", 1), ("YA", 0, 0, 2, 0), ("OC", 0), ("YA", 0, 1, 1, 1), ("CO", 0, 0, 0),
-    ("F", 0, 1, 0, "own", 1), ("SA", 0, 1, 0), ("N", 1, 4), ("F", 0, 2, 2, "own", 0), ("OY", 1, 4),
-    ("SA", 1, 0, 0), ("YA", 0, 0, 1, 0), ("YA", 0, 1, 2, 0), ("OC", 1), ("F", 0, 1, 0, "yo", 0),
-    ("F", 0, 2, 1, "own", 1), ("CO", 0, 1, 0), ("CO", 0, 1, 1), ("CO", 1, 0, 0), ("FA", 0, 0, 0),
-    ("YA", 0, 1, 1, 0), ("YS", 0, 1, 0), ("F", 0, 2, 2, "own", 1), ("YS", 0, 0, 0),
-    ("F", 0, 1, 0, "yo", 1), ("F", 0, 2, 1, "own", 0), ("YA", 0, 1, 2, 1), ("YS", 0, 1, 1),
-    ("SA", 0, 1, 1), ("OZ", 1, 4, 1), ("OY", 1, 3), ("FA", 0, 1, 0), ("F", 0, 2, 0, "own", 0),
-    ("FA", 0, 1, 1), ("F", 0, 3, 1, "own", 1), ("E", 0, 0), ("F", 0, 2, 0, "own", 1),
-    ("SA", 0, 2, 1), ("E", 0, 0), ("E", 0, 0), ("F", 0, 3, 2, "own", 0), ("F", 0, 2, 0, "yo", 0),
-    ("E", 0, 0), ("F", 0, 3, 2, "own", 1), ("OZ", 1, 4, 0), ("YA", 0, 2, 2, 0), ("E", 0, 0),
-    ("F", 0, 2, 0, "yo", 1), ("F", 0, 3, 1, "own", 0), ("YA", 1, 0, 4, 0), ("OY", 1, 5),
-    ("YA", 0, 3, 1, 1), ("YA", 0, 2, 2, 1), ("YA", 0, 2, 1, 1), ("OZ", 1, 5, 0), ("OZ", 1, 5, 1),
-    ("E", 0, 0), ("YA", 0, 2, 1, 0), ("F", 1, 1, 4, "own", 1), ("E", 0, 0), ("YA", 0, 3, 2, 0),
-    ("F", 0, 3, 0, "own", 0), ("E", 0, 0), ("CO", 0, 2, 0), ("F", 0, 3, 0, "own", 1),
-    ("CO", 0, 2, 1), ("FA", 0, 2, 1), ("YA", 0, 3, 2, 1), ("FA", 0, 2, 0), ("YA", 0, 3, 1, 0),
-    ("F", 0, 3, 0, "yo", 0), ("SA", 0, 3, 1), ("F", 0, 3, 0, "yo", 1), ("SA", 0, 3, 0),
-    ("YS", 0, 3, 1), ("CO", 0, 3, 1), ("CO", 0, 3, 0), ("SA", 0, 2, 0), ("YS", 0, 2, 0),
-    ("F", 1, 1, 4, "own", 0), ("YS", 0, 2, 1), ("FA", 0, 3, 1), ("FA", 0, 3, 0), ("YS", 0, 3, 0),
-    ("E", 0, 1), ("E", 0, 1), ("F", 1, 1, 5, "own", 1), ("OZ", 1, 3, 1), ("YA", 1, 0, 5, 0),
-    ("F", 1, 1, 5, "own", 0), ("E", 0, 1), ("E", 0, 1), ("OZ", 1, 3, 0), ("X", 1),
-    ("F", 1, 2, 4, "own", 0), ("F", 1, 2, 4, "own", 1), ("YA", 1, 1, 4, 1), ("E", 0, 1),
-    ("E", 0, 1), ("E", 0, 1), ("F", 1, 2, 5, "own", 1), ("E", 0, 1), ("AW", 0, "yo", 3, 0),
-    ("F", 1, 2, 5, "own", 0), ("AW", 0, "yy", 3, 0), ("YA", 1, 1, 4, 0), ("AW", 0, "yy", 2, 0),
-    ("F", 1, 1, 3, "own", 1), ("AW", 0, "yy", 1, 0), ("AW", 0, "yo", 3, 1), ("FA", 1, 0, 0),
-    ("AW", 0, "yy", 3, 1), ("AW", 0, "yo", 0, 0), ("AW", 0, "yo", 1, 1), ("F", 1, 1, 3, "own", 0),
-    ("SY", 0, 3, 0), ("F", 1, 1, 3, "yo", 1), ("SA", 1, 1, 1), ("YA", 1, 1, 5, 1), ("RL", 0, 3, 0),
-    ("AW", 0, "yy", 1, 1), ("YS", 1, 0, 0), ("SA", 1, 1, 0), ("F", 1, 1, 3, "yo", 0),
-    ("AW", 0, "yo", 2, 0), ("SY", 0, 3, 1), ("RL", 0, 3, 1), ("YA", 1, 1, 5, 0), ("YS", 1, 1, 1),
-    ("AW", 0, "yo", 1, 0), ("YS", 1, 1, 0), ("AW", 0, "yo", 2, 1), ("CO", 1, 1, 1),
-    ("AW", 0, "yy", 2, 1), ("CO", 1, 1, 0), ("FA", 1, 1, 1), ("FA", 1, 1, 0), ("E", 1, 0),
-    ("E", 1, 0), ("RT", 0, 3, 1, 0), ("F", 1, 3, 4, "own", 0), ("F", 1, 3, 4, "own", 1),
-    ("YA", 1, 2, 4, 0), ("RT", 0, 3, 1, 1), ("F", 1, 3, 5, "own", 1), ("SY", 0, 2, 0), ("E", 1, 0),
-    ("F", 1, 3, 5, "own", 0), ("RL", 0, 2, 0), ("SY", 0, 2, 1), ("RL", 0, 2, 1), ("YA", 1, 2, 4, 1),
-    ("F", 1, 2, 3, "own", 1), ("F", 1, 2, 3, "own", 0), ("E", 1, 0), ("YA", 1, 2, 5, 0),
-    ("E", 1, 0), ("RT", 0, 3, 2, 0), ("F", 1, 2, 3, "yo", 0), ("RT", 0, 3, 2, 1),
-    ("F", 1, 2, 3, "yo", 1), ("SY", 0, 1, 0), ("SY", 0, 1, 1), ("E", 1, 0), ("E", 1, 0),
-    ("RL", 0, 1, 0), ("YA", 1, 2, 5, 1), ("RL", 0, 1, 1), ("CO", 1, 2, 0), ("YA", 1, 3, 4, 0),
-    ("CO", 1, 2, 1), ("E", 1, 0), ("F", 1, 3, 3, "own", 1), ("F", 1, 3, 3, "own", 0),
-    ("YA", 1, 3, 4, 1), ("YA", 1, 3, 5, 1), ("SY", 0, 0, 0), ("F", 1, 3, 3, "yo", 1),
-    ("FA", 1, 2, 1), ("SA", 1, 3, 1), ("SA", 1, 3, 0), ("F", 1, 3, 3, "yo", 0), ("YA", 1, 3, 5, 0),
-    ("CO", 1, 3, 1), ("CO", 1, 3, 0), ("YS", 1, 3, 0), ("SA", 1, 2, 0), ("RT", 0, 2, 1, 0),
-    ("FA", 1, 2, 0), ("RT", 0, 2, 1, 1), ("YS", 1, 3, 1), ("YS", 1, 2, 1), ("SA", 1, 2, 1),
-    ("FA", 1, 3, 1), ("YS", 1, 2, 0), ("FA", 1, 3, 0), ("E", 1, 1), ("E", 1, 1), ("RT", 0, 2, 2, 1),
-    ("RT", 0, 2, 2, 0), ("E", 1, 1), ("E", 1, 1), ("E", 1, 1), ("E", 1, 1), ("RT", 0, 1, 1, 0),
-    ("RT", 0, 1, 1, 1), ("E", 1, 1), ("E", 1, 1), ("RT", 0, 1, 2, 1), ("AW", 1, "yo", 3, 0),
-    ("AW", 1, "yo", 3, 1), ("RT", 0, 1, 2, 0), ("AW", 1, "yy", 3, 1), ("AW", 1, "yy", 3, 0),
-    ("AW", 1, "yy", 2, 1), ("AW", 1, "yo", 2, 0), ("AW", 0, "yy", 0, 0), ("SY", 1, 3, 0),
-    ("SY", 1, 3, 1), ("RL", 1, 3, 1), ("RL", 1, 3, 0), ("AW", 1, "yy", 2, 0), ("AW", 1, "yo", 1, 0),
-    ("AW", 1, "yo", 1, 1), ("AW", 1, "yo", 2, 1), ("SY", 1, 2, 0), ("RT", 1, 3, 4, 1),
-    ("RT", 1, 3, 4, 0), ("RL", 0, 0, 0), ("RH", 0), ("SY", 1, 2, 1), ("RL", 1, 2, 1),
-    ("AW", 1, "yy", 1, 1), ("RT", 0, 0, 1, 0), ("SY", 1, 1, 0), ("AW", 1, "yo", 0, 0),
-    ("SY", 1, 1, 1), ("RT", 1, 3, 5, 0), ("AW", 1, "yy", 1, 0), ("RT", 1, 3, 5, 1), ("RL", 1, 2, 0),
-    ("RL", 1, 1, 1), ("AW", 1, "yy", 0, 0), ("RT", 1, 2, 4, 1), ("RP", 0, 1), ("RT", 0, 0, 2, 0),
-    ("RT", 1, 2, 5, 0), ("SY", 1, 0, 0), ("RT", 1, 2, 4, 0), ("RL", 1, 1, 0), ("RP", 0, 2),
-    ("RF", 0), ("RT", 1, 2, 5, 1), ("RT", 1, 1, 5, 0), ("RT", 1, 1, 4, 1), ("RT", 1, 1, 4, 0),
-    ("RT", 1, 1, 5, 1), ("RL", 1, 0, 0), ("RT", 1, 0, 4, 0), ("RH", 1), ("RT", 1, 0, 5, 0),
-    ("RP", 1, 5), ("RP", 1, 4), ("RF", 1),
+    ("P", 0), ("N", 0, 1), ("OY", 0, 1), ("N", 0, 0), ("OZ", 0, 1, 1), ("OZ", 0, 1, 0), ("N", 0, 2),
+    ("OY", 0, 2), ("OZ", 0, 2, 1), ("OZ", 0, 2, 0), ("P", 1), ("F", 0, 1, 1, "own", 1),
+    ("OZ", 0, 0, 0), ("F", 0, 1, 1, "own", 0), ("OZ", 0, 0, 1), ("OY", 0, 0),
+    ("F", 0, 1, 2, "own", 0), ("N", 1, 3), ("F", 0, 1, 2, "own", 1), ("SA", 0, 0, 0),
+    ("YA", 0, 0, 2, 0), ("N", 1, 5), ("F", 0, 1, 0, "own", 0), ("YA", 0, 1, 1, 1), ("X", 0),
+    ("F", 0, 1, 0, "own", 1), ("F", 0, 2, 1, "own", 1), ("F", 0, 2, 1, "own", 0), ("OC", 0),
+    ("CO", 0, 1, 0), ("N", 1, 4), ("YA", 0, 0, 1, 0), ("FA", 0, 0, 0), ("F", 0, 2, 2, "own", 0),
+    ("YA", 0, 1, 1, 0), ("F", 0, 2, 2, "own", 1), ("CO", 0, 0, 0), ("F", 0, 1, 0, "yo", 1),
+    ("OY", 1, 4), ("SA", 0, 1, 0), ("YA", 0, 1, 2, 0), ("SA", 1, 0, 0), ("OC", 1),
+    ("F", 0, 1, 0, "yo", 0), ("YS", 0, 1, 0), ("YS", 0, 0, 0), ("F", 0, 2, 0, "own", 1),
+    ("OY", 1, 3), ("SA", 0, 1, 1), ("F", 0, 2, 0, "own", 0), ("YA", 0, 1, 2, 1), ("YS", 0, 1, 1),
+    ("F", 0, 3, 1, "own", 0), ("CO", 0, 2, 1), ("F", 0, 3, 1, "own", 1), ("CO", 0, 1, 1),
+    ("FA", 0, 1, 0), ("CO", 1, 0, 0), ("OZ", 1, 4, 1), ("FA", 0, 1, 1), ("SA", 0, 2, 0),
+    ("E", 0, 0), ("OZ", 1, 4, 0), ("E", 0, 0), ("E", 0, 0), ("F", 0, 3, 2, "own", 0),
+    ("CO", 0, 2, 0), ("F", 0, 3, 2, "own", 1), ("YA", 0, 2, 2, 0), ("E", 0, 0), ("OY", 1, 5),
+    ("YA", 0, 2, 2, 1), ("F", 0, 2, 0, "yo", 1), ("F", 0, 2, 0, "yo", 0), ("OZ", 1, 5, 1),
+    ("YA", 0, 2, 1, 1), ("YA", 0, 2, 1, 0), ("OZ", 1, 5, 0), ("E", 0, 0), ("SA", 0, 2, 1),
+    ("E", 0, 0), ("E", 0, 0), ("E", 0, 0), ("YA", 0, 3, 1, 1), ("YA", 1, 0, 4, 0),
+    ("F", 1, 1, 4, "own", 1), ("F", 0, 3, 0, "own", 0), ("YA", 0, 3, 1, 0),
+    ("F", 0, 3, 0, "own", 1), ("FA", 0, 2, 0), ("F", 1, 1, 4, "own", 0), ("SA", 0, 3, 1),
+    ("SA", 0, 3, 0), ("YA", 0, 3, 2, 0), ("YA", 0, 3, 2, 1), ("F", 0, 3, 0, "yo", 0),
+    ("YS", 0, 3, 0), ("FA", 0, 2, 1), ("F", 0, 3, 0, "yo", 1), ("YS", 0, 3, 1), ("CO", 0, 3, 1),
+    ("CO", 0, 3, 0), ("YS", 0, 2, 0), ("FA", 0, 3, 0), ("YS", 0, 2, 1), ("FA", 0, 3, 1),
+    ("E", 0, 1), ("E", 0, 1), ("F", 1, 1, 5, "own", 0), ("F", 1, 1, 5, "own", 1), ("OZ", 1, 3, 0),
+    ("E", 0, 1), ("OZ", 1, 3, 1), ("YA", 1, 0, 5, 0), ("X", 1), ("E", 0, 1), ("YS", 1, 0, 0),
+    ("YA", 1, 1, 4, 1), ("F", 1, 2, 4, "own", 0), ("E", 0, 1), ("F", 1, 2, 4, "own", 1),
+    ("E", 0, 1), ("E", 0, 1), ("F", 1, 2, 5, "own", 0), ("F", 1, 2, 5, "own", 1), ("E", 0, 1),
+    ("AW", 0, "yo", 3, 0), ("AW", 0, "yo", 3, 1), ("AW", 0, "yo", 2, 1), ("AW", 0, "yy", 3, 1),
+    ("F", 1, 1, 3, "own", 0), ("YA", 1, 1, 5, 0), ("AW", 0, "yy", 3, 0), ("FA", 1, 0, 0),
+    ("AW", 0, "yo", 1, 1), ("YA", 1, 1, 4, 0), ("F", 1, 1, 3, "own", 1), ("SY", 0, 3, 1),
+    ("AW", 0, "yo", 2, 0), ("F", 1, 1, 3, "yo", 0), ("SA", 1, 1, 1), ("SA", 1, 1, 0),
+    ("SY", 0, 3, 0), ("AW", 0, "yy", 2, 1), ("YA", 1, 1, 5, 1), ("F", 1, 1, 3, "yo", 1),
+    ("YS", 1, 1, 1), ("RL", 0, 3, 0), ("YS", 1, 1, 0), ("AW", 0, "yy", 1, 0), ("AW", 0, "yy", 1, 1),
+    ("RL", 0, 3, 1), ("AW", 0, "yy", 2, 0), ("YA", 1, 2, 4, 0), ("CO", 1, 1, 0), ("FA", 1, 1, 0),
+    ("F", 1, 3, 4, "own", 0), ("CO", 1, 1, 1), ("F", 1, 3, 4, "own", 1), ("FA", 1, 1, 1),
+    ("E", 1, 0), ("E", 1, 0), ("RT", 0, 3, 1, 1), ("RT", 0, 3, 1, 0), ("YA", 1, 2, 5, 1),
+    ("YA", 1, 2, 4, 1), ("E", 1, 0), ("F", 1, 3, 5, "own", 0), ("F", 1, 3, 5, "own", 1),
+    ("YA", 1, 2, 5, 0), ("SY", 0, 2, 0), ("RL", 0, 2, 0), ("AW", 0, "yo", 0, 0),
+    ("AW", 0, "yo", 1, 0), ("SY", 0, 2, 1), ("F", 1, 2, 3, "own", 1), ("RL", 0, 2, 1),
+    ("F", 1, 2, 3, "own", 0), ("E", 1, 0), ("E", 1, 0), ("RT", 0, 3, 2, 1), ("RT", 0, 3, 2, 0),
+    ("F", 1, 2, 3, "yo", 0), ("F", 1, 2, 3, "yo", 1), ("SY", 0, 1, 1), ("CO", 1, 2, 0), ("E", 1, 0),
+    ("YS", 1, 2, 1), ("E", 1, 0), ("SY", 0, 1, 0), ("YA", 1, 3, 4, 1), ("RL", 0, 1, 0),
+    ("F", 1, 3, 3, "own", 1), ("YA", 1, 3, 4, 0), ("SY", 0, 0, 0), ("E", 1, 0), ("CO", 1, 3, 1),
+    ("YA", 1, 3, 5, 1), ("F", 1, 3, 3, "own", 0), ("YA", 1, 3, 5, 0), ("F", 1, 3, 3, "yo", 1),
+    ("FA", 1, 2, 0), ("RL", 0, 1, 1), ("SA", 1, 2, 1), ("SA", 1, 3, 1), ("SA", 1, 2, 0),
+    ("RT", 0, 2, 1, 0), ("FA", 1, 2, 1), ("CO", 1, 2, 1), ("YS", 1, 3, 1), ("F", 1, 3, 3, "yo", 0),
+    ("SA", 1, 3, 0), ("YS", 1, 3, 0), ("CO", 1, 3, 0), ("RT", 0, 2, 1, 1), ("YS", 1, 2, 0),
+    ("FA", 1, 3, 1), ("FA", 1, 3, 0), ("E", 1, 1), ("E", 1, 1), ("RT", 0, 2, 2, 0), ("E", 1, 1),
+    ("RT", 0, 2, 2, 1), ("E", 1, 1), ("E", 1, 1), ("E", 1, 1), ("RT", 0, 1, 1, 0),
+    ("RT", 0, 1, 1, 1), ("E", 1, 1), ("E", 1, 1), ("AW", 1, "yo", 3, 1), ("AW", 1, "yo", 2, 1),
+    ("RT", 0, 1, 2, 0), ("AW", 1, "yo", 3, 0), ("AW", 1, "yo", 1, 1), ("RT", 0, 1, 2, 1),
+    ("AW", 1, "yy", 3, 1), ("AW", 1, "yy", 3, 0), ("AW", 1, "yo", 2, 0), ("SY", 1, 3, 1),
+    ("AW", 1, "yo", 0, 0), ("SY", 1, 3, 0), ("RL", 1, 3, 0), ("AW", 1, "yy", 2, 0),
+    ("AW", 1, "yy", 2, 1), ("SY", 1, 2, 0), ("AW", 1, "yy", 1, 0), ("AW", 1, "yy", 1, 1),
+    ("AW", 1, "yy", 0, 0), ("RL", 1, 3, 1), ("RT", 1, 3, 4, 1), ("AW", 1, "yo", 1, 0),
+    ("SY", 1, 2, 1), ("RL", 1, 2, 0), ("RT", 1, 3, 5, 1), ("SY", 1, 1, 1), ("AW", 0, "yy", 0, 0),
+    ("RL", 0, 0, 0), ("RL", 1, 2, 1), ("RT", 1, 2, 5, 1), ("SY", 1, 1, 0), ("RT", 0, 0, 2, 0),
+    ("RP", 0, 2), ("RH", 0), ("RT", 1, 3, 4, 0), ("RT", 1, 2, 4, 1), ("RT", 1, 3, 5, 0),
+    ("RT", 1, 2, 4, 0), ("RT", 1, 2, 5, 0), ("RL", 1, 1, 0), ("RL", 1, 1, 1), ("RT", 1, 1, 4, 0),
+    ("SY", 1, 0, 0), ("RT", 0, 0, 1, 0), ("RT", 1, 1, 5, 1), ("RT", 1, 1, 5, 0), ("RP", 0, 1),
+    ("RF", 0), ("RT", 1, 1, 4, 1), ("RL", 1, 0, 0), ("RH", 1), ("RT", 1, 0, 5, 0),
+    ("RT", 1, 0, 4, 0), ("RP", 1, 5), ("RP", 1, 4), ("RF", 1),
 )
 MESH = pl.DeviceIdType.MESH
 
@@ -296,13 +297,13 @@
                 c.wait()
 
         def project(i, carry):
-            at = pl.ds(pl.multiple_of(i * 1024, 1024), 1024)
+            at = pl.ds(pl.multiple_of(i * width, width), width)
             mix[rows_h[h], at] = jnp.dot(
-                pooled[rows_h[h]], from_core[:, :, :, at].reshape(pooled.shape[1], 1024),
+                pooled[rows_h[h]], from_core[:, :, :, at].reshape(pooled.shape[1], width),
                 preferred_element_type=jnp.float32)
             return carry
 
-        lax.fori_loop(0, width // 1024, project, 0)
+        project(0, 0)
 
     def norm_rows(part):
         begin, count = cuts[part][:2]
@@ -662,6 +663,11 @@
             over_core(h, far_core, *at)
         elif kind == "W":
             sent_all(h)
+        elif kind == "WP":
+            pl.when(has_next)(lambda: halo(tp).wait_send())
+            each_spread(lambda c: c.wait_send())
+        elif kind == "WR":
+            reduce_sent(h)
         elif kind == "M":
             for number, by in enumerate(others):
                 meta_copy(number, by).wait()
@@ -686,13 +692,15 @@
 
     todo, waited = [], set()
     for one in ORDER:
-        if one[0] == "AW" and one[1] not in waited:
-            waited.add(one[1])
-            todo.append(("W", one[1]))
         if one[0] in ("SA", "YS", "CO", "FA") and "M" not in waited:
             waited.add("M")
             todo.append(("M", 0))
         todo.append(one)
+    late = [i for i, one in enumerate(todo) if one[:2] == ("RT", 1)]
+    todo.insert(late[len(late) * 2 // 3] + 1, ("W", 1))
+    todo.insert(late[len(late) // 3] + 1, ("W", 0))
+    todo.insert(late[0] + 1, ("WP", 0))
+    todo.insert(todo.index(("RF", 0)) + 1, ("WR", 0))
     while todo:
         one = todo.pop(0)
         if one[0] != "E":
@@ -708,10 +716,7 @@
             else:
                 between.append((seen, [one]))
         experts(h, far, between)
-    reduce_sent(0)
     reduce_sent(1)
-    pl.when(has_next)(lambda: halo(tp).wait_send())
-    each_spread(lambda c: c.wait_send())
 
 
 def cut_rows(halves):

time: 106 us -> 105 us (level)
    pallas_call x1, Pallas kernels: 104 us -> 103 us  [fused_layer(): pl.pallas_call(functools.partial(layer_kernel, n_tp, cuts, rcuts), out_sh...]
where the time goes in v4:
time: 105 us
  Pallas kernels  103 us (98%)
  local copies, waits for them, and re-layouts  1.88 us (2%)
    pallas_call x1, Pallas kernels, fused_layer(): pl.pallas_call(functools.partial(layer_kernel, n_tp, cuts, rcuts), out_sh...  103 us

profile of v4, /device:TPU:0, one launch (start us, length us, event | category | flops | bytes accessed | tf_op | source)
XLA Modules:
  0.0 104.8 jit_solution(12830347340059310762)
XLA Ops:
  0.0 102.9 %fused_layer.1 = bf16[128,2048]{1,0:T(8,128)(2,1)} custom-call(bf16[512,256]{1,0:T(8,128)(2,1)} %pool_ref.1, bf16[4,256,256]{2,1,0:T(8,128)(2,1)} %pw_ref.1, f32[1,1024]{1,0:T(1,128)} %bitcast.9, bf16[1024,2048]{1,0:T(8,128)(2,1)} %ow_ref.1, bf16[128,2048]{1,0:T(8,128)(2,1)} %resid_ref.1, f32[1,2048]{1,0:T(1,128)} %bitcast.6, f32[1,2048]{1,0:T(1,128)} %bitcast.7, ...), custom_call_target="tpu_custom_call" | custom-call | tf_op jit(solution)/shard_map/fused_layer/pallas_call | solution.py:774
  103.0 1.9 %copy.15 = bf16[128,2048]{1,0:T(8,128)(2,1)} copy(bf16[128,2048]{1,0:T(8,128)(2,1)} %fused_layer.1) | data formatting | bytes 1048576

commit v5 on v4

--- a/solution.py
+++ b/solution.py
@@ -38,71 +38,70 @@
 
 
 SLOT = 16
-HALVES = ((16, 16, 32), (16, 16, 32))
+HALVES = ((16, 32, 16), (16, 16, 32))
 BACK = ((16, 16, 32), (16, 16, 32))
 ORDER = (
-    ("P", 0), ("N", 0, 1), ("OY", 0, 1), ("N", 0, 0), ("OZ", 0, 1, 1), ("OZ", 0, 1, 0), ("N", 0, 2),
-    ("OY", 0, 2), ("OZ", 0, 2, 1), ("OZ", 0, 2, 0), ("P", 1), ("F", 0, 1, 1, "own", 1),
-    ("OZ", 0, 0, 0), ("F", 0, 1, 1, "own", 0), ("OZ", 0, 0, 1), ("OY", 0, 0),
-    ("F", 0, 1, 2, "own", 0), ("N", 1, 3), ("F", 0, 1, 2, "own", 1), ("SA", 0, 0, 0),
-    ("YA", 0, 0, 2, 0), ("N", 1, 5), ("F", 0, 1, 0, "own", 0), ("YA", 0, 1, 1, 1), ("X", 0),
-    ("F", 0, 1, 0, "own", 1), ("F", 0, 2, 1, "own", 1), ("F", 0, 2, 1, "own", 0), ("OC", 0),
-    ("CO", 0, 1, 0), ("N", 1, 4), ("YA", 0, 0, 1, 0), ("FA", 0, 0, 0), ("F", 0, 2, 2, "own", 0),
-    ("YA", 0, 1, 1, 0), ("F", 0, 2, 2, "own", 1), ("CO", 0, 0, 0), ("F", 0, 1, 0, "yo", 1),
-    ("OY", 1, 4), ("SA", 0, 1, 0), ("YA", 0, 1, 2, 0), ("SA", 1, 0, 0), ("OC", 1),
-    ("F", 0, 1, 0, "yo", 0), ("YS", 0, 1, 0), ("YS", 0, 0, 0), ("F", 0, 2, 0, "own", 1),
-    ("OY", 1, 3), ("SA", 0, 1, 1), ("F", 0, 2, 0, "own", 0), ("YA", 0, 1, 2, 1), ("YS", 0, 1, 1),
-    ("F", 0, 3, 1, "own", 0), ("CO", 0, 2, 1), ("F", 0, 3, 1, "own", 1), ("CO", 0, 1, 1),
-    ("FA", 0, 1, 0), ("CO", 1, 0, 0), ("OZ", 1, 4, 1), ("FA", 0, 1, 1), ("SA", 0, 2, 0),
-    ("E", 0, 0), ("OZ", 1, 4, 0), ("E", 0, 0), ("E", 0, 0), ("F", 0, 3, 2, "own", 0),
-    ("CO", 0, 2, 0), ("F", 0, 3, 2, "own", 1), ("YA", 0, 2, 2, 0), ("E", 0, 0), ("OY", 1, 5),
-    ("YA", 0, 2, 2, 1), ("F", 0, 2, 0, "yo", 1), ("F", 0, 2, 0, "yo", 0), ("OZ", 1, 5, 1),
-    ("YA", 0, 2, 1, 1), ("YA", 0, 2, 1, 0), ("OZ", 1, 5, 0), ("E", 0, 0), ("SA", 0, 2, 1),
-    ("E", 0, 0), ("E", 0, 0), ("E", 0, 0), ("YA", 0, 3, 1, 1), ("YA", 1, 0, 4, 0),
-    ("F", 1, 1, 4, "own", 1), ("F", 0, 3, 0, "own", 0), ("YA", 0, 3, 1, 0),
-    ("F", 0, 3, 0, "own", 1), ("FA", 0, 2, 0), ("F", 1, 1, 4, "own", 0), ("SA", 0, 3, 1),
-    ("SA", 0, 3, 0), ("YA", 0, 3, 2, 0), ("YA", 0, 3, 2, 1), ("F", 0, 3, 0, "yo", 0),
-    ("YS", 0, 3, 0), ("FA", 0, 2, 1), ("F", 0, 3, 0, "yo", 1), ("YS", 0, 3, 1), ("CO", 0, 3, 1),
-    ("CO", 0, 3, 0), ("YS", 0, 2, 0), ("FA", 0, 3, 0), ("YS", 0, 2, 1), ("FA", 0, 3, 1),
-    ("E", 0, 1), ("E", 0, 1), ("F", 1, 1, 5, "own", 0), ("F", 1, 1, 5, "own", 1), ("OZ", 1, 3, 0),
-    ("E", 0, 1), ("OZ", 1, 3, 1), ("YA", 1, 0, 5, 0), ("X", 1), ("E", 0, 1), ("YS", 1, 0, 0),
-    ("YA", 1, 1, 4, 1), ("F", 1, 2, 4, "own", 0), ("E", 0, 1), ("F", 1, 2, 4, "own", 1),
-    ("E", 0, 1), ("E", 0, 1), ("F", 1, 2, 5, "own", 0), ("F", 1, 2, 5, "own", 1), ("E", 0, 1),
-    ("AW", 0, "yo", 3, 0), ("AW", 0, "yo", 3, 1), ("AW", 0, "yo", 2, 1), ("AW", 0, "yy", 3, 1),
-    ("F", 1, 1, 3, "own", 0), ("YA", 1, 1, 5, 0), ("AW", 0, "yy", 3, 0), ("FA", 1, 0, 0),
-    ("AW", 0, "yo", 1, 1), ("YA", 1, 1, 4, 0), ("F", 1, 1, 3, "own", 1), ("SY", 0, 3, 1),
-    ("AW", 0, "yo", 2, 0), ("F", 1, 1, 3, "yo", 0), ("SA", 1, 1, 1), ("SA", 1, 1, 0),
-    ("SY", 0, 3, 0), ("AW", 0, "yy", 2, 1), ("YA", 1, 1, 5, 1), ("F", 1, 1, 3, "yo", 1),
-    ("YS", 1, 1, 1), ("RL", 0, 3, 0), ("YS", 1, 1, 0), ("AW", 0, "yy", 1, 0), ("AW", 0, "yy", 1, 1),
-    ("RL", 0, 3, 1), ("AW", 0, "yy", 2, 0), ("YA", 1, 2, 4, 0), ("CO", 1, 1, 0), ("FA", 1, 1, 0),
-    ("F", 1, 3, 4, "own", 0), ("CO", 1, 1, 1), ("F", 1, 3, 4, "own", 1), ("FA", 1, 1, 1),
-    ("E", 1, 0), ("E", 1, 0), ("RT", 0, 3, 1, 1), ("RT", 0, 3, 1, 0), ("YA", 1, 2, 5, 1),
-    ("YA", 1, 2, 4, 1), ("E", 1, 0), ("F", 1, 3, 5, "own", 0), ("F", 1, 3, 5, "own", 1),
-    ("YA", 1, 2, 5, 0), ("SY", 0, 2, 0), ("RL", 0, 2, 0), ("AW", 0, "yo", 0, 0),
-    ("AW", 0, "yo", 1, 0), ("SY", 0, 2, 1), ("F", 1, 2, 3, "own", 1), ("RL", 0, 2, 1),
-    ("F", 1, 2, 3, "own", 0), ("E", 1, 0), ("E", 1, 0), ("RT", 0, 3, 2, 1), ("RT", 0, 3, 2, 0),
-    ("F", 1, 2, 3, "yo", 0), ("F", 1, 2, 3, "yo", 1), ("SY", 0, 1, 1), ("CO", 1, 2, 0), ("E", 1, 0),
-    ("YS", 1, 2, 1), ("E", 1, 0), ("SY", 0, 1, 0), ("YA", 1, 3, 4, 1), ("RL", 0, 1, 0),
-    ("F", 1, 3, 3, "own", 1), ("YA", 1, 3, 4, 0), ("SY", 0, 0, 0), ("E", 1, 0), ("CO", 1, 3, 1),
-    ("YA", 1, 3, 5, 1), ("F", 1, 3, 3, "own", 0), ("YA", 1, 3, 5, 0), ("F", 1, 3, 3, "yo", 1),
-    ("FA", 1, 2, 0), ("RL", 0, 1, 1), ("SA", 1, 2, 1), ("SA", 1, 3, 1), ("SA", 1, 2, 0),
-    ("RT", 0, 2, 1, 0), ("FA", 1, 2, 1), ("CO", 1, 2, 1), ("YS", 1, 3, 1), ("F", 1, 3, 3, "yo", 0),
-    ("SA", 1, 3, 0), ("YS", 1, 3, 0), ("CO", 1, 3, 0), ("RT", 0, 2, 1, 1), ("YS", 1, 2, 0),
-    ("FA", 1, 3, 1), ("FA", 1, 3, 0), ("E", 1, 1), ("E", 1, 1), ("RT", 0, 2, 2, 0), ("E", 1, 1),
-    ("RT", 0, 2, 2, 1), ("E", 1, 1), ("E", 1, 1), ("E", 1, 1), ("RT", 0, 1, 1, 0),
-    ("RT", 0, 1, 1, 1), ("E", 1, 1), ("E", 1, 1), ("AW", 1, "yo", 3, 1), ("AW", 1, "yo", 2, 1),
-    ("RT", 0, 1, 2, 0), ("AW", 1, "yo", 3, 0), ("AW", 1, "yo", 1, 1), ("RT", 0, 1, 2, 1),
-    ("AW", 1, "yy", 3, 1), ("AW", 1, "yy", 3, 0), ("AW", 1, "yo", 2, 0), ("SY", 1, 3, 1),
-    ("AW", 1, "yo", 0, 0), ("SY", 1, 3, 0), ("RL", 1, 3, 0), ("AW", 1, "yy", 2, 0),
-    ("AW", 1, "yy", 2, 1), ("SY", 1, 2, 0), ("AW", 1, "yy", 1, 0), ("AW", 1, "yy", 1, 1),
-    ("AW", 1, "yy", 0, 0), ("RL", 1, 3, 1), ("RT", 1, 3, 4, 1), ("AW", 1, "yo", 1, 0),
-    ("SY", 1, 2, 1), ("RL", 1, 2, 0), ("RT", 1, 3, 5, 1), ("SY", 1, 1, 1), ("AW", 0, "yy", 0, 0),
-    ("RL", 0, 0, 0), ("RL", 1, 2, 1), ("RT", 1, 2, 5, 1), ("SY", 1, 1, 0), ("RT", 0, 0, 2, 0),
-    ("RP", 0, 2), ("RH", 0), ("RT", 1, 3, 4, 0), ("RT", 1, 2, 4, 1), ("RT", 1, 3, 5, 0),
-    ("RT", 1, 2, 4, 0), ("RT", 1, 2, 5, 0), ("RL", 1, 1, 0), ("RL", 1, 1, 1), ("RT", 1, 1, 4, 0),
-    ("SY", 1, 0, 0), ("RT", 0, 0, 1, 0), ("RT", 1, 1, 5, 1), ("RT", 1, 1, 5, 0), ("RP", 0, 1),
-    ("RF", 0), ("RT", 1, 1, 4, 1), ("RL", 1, 0, 0), ("RH", 1), ("RT", 1, 0, 5, 0),
-    ("RT", 1, 0, 4, 0), ("RP", 1, 5), ("RP", 1, 4), ("RF", 1),
+    ("P", 0), ("N", 0, 2), ("OZ", 0, 2, 1), ("OY", 0, 2), ("OZ", 0, 2, 0), ("N", 0, 0),
+    ("OZ", 0, 0, 1), ("OY", 0, 0), ("N", 0, 1), ("OZ", 0, 1, 0), ("OZ", 0, 0, 0), ("OC", 0),
+    ("OY", 0, 1), ("OZ", 0, 1, 1), ("F", 0, 1, 2, "own", 0), ("P", 1), ("F", 0, 1, 2, "own", 1),
+    ("F", 0, 1, 1, "own", 0), ("X", 0), ("F", 0, 1, 0, "own", 0), ("YA", 0, 0, 2, 0),
+    ("F", 0, 1, 1, "own", 1), ("F", 0, 1, 0, "own", 1), ("N", 1, 5), ("N", 1, 4),
+    ("F", 0, 2, 2, "own", 0), ("SA", 0, 1, 0), ("OY", 1, 4), ("N", 1, 3), ("F", 0, 1, 0, "yo", 1),
+    ("CO", 0, 1, 0), ("SA", 0, 1, 1), ("YA", 0, 1, 2, 1), ("SA", 1, 0, 0), ("YA", 0, 0, 1, 0),
+    ("YA", 0, 1, 2, 0), ("OC", 1), ("CO", 0, 1, 1), ("F", 0, 2, 2, "own", 1),
+    ("F", 0, 2, 1, "own", 0), ("CO", 0, 0, 0), ("YA", 0, 1, 1, 0), ("F", 0, 1, 0, "yo", 0),
+    ("YS", 0, 0, 0), ("FA", 0, 0, 0), ("FA", 0, 1, 0), ("YS", 0, 1, 0), ("F", 0, 2, 0, "own", 0),
+    ("OZ", 1, 4, 0), ("SA", 0, 0, 0), ("YA", 0, 1, 1, 1), ("F", 0, 2, 1, "own", 1), ("YS", 0, 1, 1),
+    ("F", 0, 2, 0, "yo", 1), ("F", 0, 2, 0, "own", 1), ("OY", 1, 3), ("OZ", 1, 5, 1),
+    ("FA", 0, 1, 1), ("E", 0, 0), ("E", 0, 0), ("OZ", 1, 4, 1), ("E", 0, 0),
+    ("F", 0, 3, 2, "own", 0), ("YA", 0, 2, 2, 1), ("F", 0, 3, 2, "own", 1), ("E", 0, 0),
+    ("CO", 0, 2, 1), ("F", 0, 3, 1, "own", 1), ("F", 0, 3, 1, "own", 0), ("CO", 1, 0, 0),
+    ("E", 0, 0), ("YA", 0, 2, 2, 0), ("YA", 0, 2, 1, 1), ("F", 0, 2, 0, "yo", 0), ("CO", 0, 2, 0),
+    ("YA", 0, 3, 2, 0), ("OY", 1, 5), ("SA", 0, 2, 0), ("YA", 0, 2, 1, 0), ("OZ", 1, 5, 0),
+    ("E", 0, 0), ("F", 0, 3, 0, "own", 0), ("E", 0, 0), ("FA", 0, 2, 1), ("SA", 0, 2, 1),
+    ("F", 0, 3, 0, "own", 1), ("FA", 0, 2, 0), ("YA", 0, 3, 2, 1), ("YS", 0, 2, 1),
+    ("F", 1, 1, 4, "own", 0), ("CO", 0, 3, 0), ("F", 0, 3, 0, "yo", 1), ("YA", 0, 3, 1, 0),
+    ("E", 0, 0), ("YA", 0, 3, 1, 1), ("SA", 0, 3, 1), ("CO", 0, 3, 1), ("YS", 0, 3, 1),
+    ("F", 0, 3, 0, "yo", 0), ("YS", 0, 2, 0), ("YA", 1, 0, 4, 0), ("YS", 0, 3, 0),
+    ("F", 1, 1, 5, "own", 1), ("SA", 0, 3, 0), ("FA", 0, 3, 1), ("FA", 0, 3, 0), ("OZ", 1, 3, 1),
+    ("E", 0, 1), ("E", 0, 1), ("F", 1, 1, 4, "own", 1), ("F", 1, 1, 5, "own", 0), ("OZ", 1, 3, 0),
+    ("X", 1), ("E", 0, 1), ("E", 0, 1), ("YA", 1, 0, 5, 0), ("E", 0, 1),
+    ("F", 1, 2, 4, "own", 0), ("F", 1, 2, 5, "own", 1), ("E", 0, 1), ("E", 0, 1), ("E", 0, 1),
+    ("YA", 1, 1, 5, 1), ("F", 1, 2, 5, "own", 0), ("AW", 0, "yo", 3, 1), ("AW", 0, "yo", 3, 0),
+    ("AW", 0, "yy", 3, 1), ("F", 1, 2, 4, "own", 1), ("AW", 0, "yy", 3, 0), ("AW", 0, "yo", 2, 1),
+    ("FA", 1, 0, 0), ("YA", 1, 1, 4, 0), ("AW", 0, "yy", 1, 0), ("AW", 0, "yo", 2, 0),
+    ("AW", 0, "yo", 1, 1), ("F", 1, 1, 3, "own", 0), ("F", 1, 1, 3, "own", 1), ("SY", 0, 3, 0),
+    ("YA", 1, 1, 4, 1), ("YS", 1, 0, 0), ("F", 1, 1, 3, "yo", 1), ("YA", 1, 1, 5, 0),
+    ("SY", 0, 3, 1), ("F", 1, 1, 3, "yo", 0), ("YS", 1, 1, 0), ("RL", 0, 3, 1), ("RL", 0, 3, 0),
+    ("AW", 0, "yy", 1, 1), ("YS", 1, 1, 1), ("SA", 1, 1, 0), ("AW", 0, "yy", 2, 0), ("SA", 1, 1, 1),
+    ("CO", 1, 1, 1), ("CO", 1, 1, 0), ("FA", 1, 1, 1), ("FA", 1, 1, 0), ("AW", 0, "yy", 2, 1),
+    ("E", 1, 0), ("E", 1, 0), ("RT", 0, 3, 1, 0), ("F", 1, 3, 5, "own", 1), ("YA", 1, 2, 5, 0),
+    ("F", 1, 3, 4, "own", 1), ("RT", 0, 3, 1, 1), ("SY", 0, 2, 0), ("F", 1, 3, 4, "own", 0),
+    ("F", 1, 3, 5, "own", 0), ("RL", 0, 2, 0), ("SY", 0, 2, 1), ("RL", 0, 2, 1), ("YA", 1, 2, 4, 1),
+    ("E", 1, 0), ("F", 1, 2, 3, "own", 1), ("F", 1, 2, 3, "own", 0), ("AW", 0, "yo", 0, 0),
+    ("E", 1, 0), ("RT", 0, 3, 2, 0), ("E", 1, 0), ("F", 1, 2, 3, "yo", 1), ("RT", 0, 3, 2, 1),
+    ("AW", 0, "yo", 1, 0), ("F", 1, 2, 3, "yo", 0), ("E", 1, 0), ("SY", 0, 1, 1), ("E", 1, 0),
+    ("RL", 0, 1, 1), ("SA", 1, 2, 0), ("YA", 1, 2, 5, 1), ("SY", 0, 1, 0), ("YA", 1, 3, 5, 1),
+    ("YA", 1, 2, 4, 0), ("SY", 0, 0, 0), ("F", 1, 3, 3, "own", 0), ("RL", 0, 1, 0), ("E", 1, 0),
+    ("YA", 1, 3, 5, 0), ("FA", 1, 2, 0), ("CO", 1, 2, 1), ("F", 1, 3, 3, "own", 1), ("SA", 1, 3, 1),
+    ("FA", 1, 2, 1), ("F", 1, 3, 3, "yo", 1), ("YA", 1, 3, 4, 0), ("YS", 1, 2, 0),
+    ("YA", 1, 3, 4, 1), ("F", 1, 3, 3, "yo", 0), ("CO", 1, 3, 0), ("SA", 1, 2, 1), ("YS", 1, 3, 1),
+    ("SA", 1, 3, 0), ("RT", 0, 2, 1, 0), ("CO", 1, 3, 1), ("YS", 1, 2, 1), ("CO", 1, 2, 0),
+    ("FA", 1, 3, 1), ("RT", 0, 2, 1, 1), ("YS", 1, 3, 0), ("FA", 1, 3, 0), ("E", 1, 1), ("E", 1, 1),
+    ("RT", 0, 2, 2, 0), ("RT", 0, 2, 2, 1), ("E", 1, 1), ("E", 1, 1), ("RT", 0, 1, 1, 0),
+    ("RT", 0, 1, 1, 1), ("E", 1, 1), ("E", 1, 1), ("E", 1, 1), ("RT", 0, 1, 2, 0), ("E", 1, 1),
+    ("AW", 1, "yo", 3, 0), ("AW", 1, "yy", 3, 0), ("AW", 1, "yo", 2, 0), ("AW", 1, "yy", 2, 0),
+    ("RT", 0, 1, 2, 1), ("AW", 1, "yo", 3, 1), ("AW", 1, "yy", 3, 1), ("AW", 1, "yo", 2, 1),
+    ("AW", 1, "yy", 2, 1), ("AW", 0, "yy", 0, 0), ("SY", 1, 3, 1), ("SY", 1, 3, 0), ("RL", 1, 3, 1),
+    ("AW", 1, "yo", 1, 1), ("RL", 1, 3, 0), ("SY", 1, 2, 1), ("AW", 1, "yy", 1, 0),
+    ("AW", 1, "yy", 1, 1), ("RL", 1, 2, 1), ("RT", 1, 3, 5, 1), ("AW", 1, "yo", 1, 0),
+    ("AW", 1, "yo", 0, 0), ("RT", 1, 3, 4, 1), ("SY", 1, 2, 0), ("RL", 1, 2, 0), ("SY", 1, 1, 1),
+    ("RT", 1, 3, 4, 0), ("SY", 1, 1, 0), ("RL", 0, 0, 0), ("RH", 0), ("RT", 0, 0, 2, 0),
+    ("RP", 0, 2), ("RT", 1, 2, 5, 1), ("AW", 1, "yy", 0, 0), ("RT", 1, 3, 5, 0), ("SY", 1, 0, 0),
+    ("RT", 1, 2, 4, 0), ("RT", 1, 2, 5, 0), ("RT", 1, 2, 4, 1), ("RL", 1, 1, 1), ("RL", 1, 1, 0),
+    ("RL", 1, 0, 0), ("RT", 1, 1, 5, 1), ("RT", 0, 0, 1, 0), ("RT", 1, 1, 5, 0), ("RT", 1, 1, 4, 1),
+    ("RT", 1, 1, 4, 0), ("RH", 1), ("RP", 0, 1), ("RT", 1, 0, 5, 0), ("RP", 1, 5), ("RF", 0),
+    ("RT", 1, 0, 4, 0), ("RP", 1, 4), ("RF", 1),
 )
 MESH = pl.DeviceIdType.MESH
 

time: 105 us -> 104 us (level)
  no operation moved by 1% of the time
where the time goes in v5:
time: 104 us
  Pallas kernels  102 us (98%)
  local copies, waits for them, and re-layouts  1.88 us (2%)
    pallas_call x1, Pallas kernels, fused_layer(): pl.pallas_call(functools.partial(layer_kernel, n_tp, cuts, rcuts), out_sh...  102 us

profile of v5, /device:TPU:0, one launch (start us, length us, event | category | flops | bytes accessed | tf_op | source)
XLA Modules:
  0.0 104.2 jit_solution(13613863743554963722)
XLA Ops:
  0.0 102.4 %fused_layer.1 = bf16[128,2048]{1,0:T(8,128)(2,1)} custom-call(bf16[512,256]{1,0:T(8,128)(2,1)} %pool_ref.1, bf16[4,256,256]{2,1,0:T(8,128)(2,1)} %pw_ref.1, f32[1,1024]{1,0:T(1,128)} %bitcast.9, bf16[1024,2048]{1,0:T(8,128)(2,1)} %ow_ref.1, bf16[128,2048]{1,0:T(8,128)(2,1)} %resid_ref.1, f32[1,2048]{1,0:T(1,128)} %bitcast.6, f32[1,2048]{1,0:T(1,128)} %bitcast.7, ...), custom_call_target="tpu_custom_call" | custom-call | tf_op jit(solution)/shard_map/fused_layer/pallas_call | solution.py:773
  102.4 1.9 %copy.15 = bf16[128,2048]{1,0:T(8,128)(2,1)} copy(bf16[128,2048]{1,0:T(8,128)(2,1)} %fused_layer.1) | data formatting | bytes 1048576
